TPU v7x, 32 devices: a whole 2x2x4 slice. The times are simulated.
32 devices in a mesh: rep: 2 (over x), fs: 8 (over z, y), tp: 2 (over core).
Axes of the slice: x: 2, y: 2, z: 4, core: 2. Of those that a mesh axis runs over, the one named last changes fastest.
Arguments:
- tokens: bfloat16 [16, 512, 2048], P(('rep', 'fs'), 'tp'), may hold values from -6 to 6
- norm_first: bfloat16 [2048], replicated, may hold values from 0.099609375 to 1.8984375
- norm_mixer: bfloat16 [2048], replicated, may hold values from 0.099609375 to 1.8984375
- norm_second: bfloat16 [2048], replicated, may hold values from 0.099609375 to 1.8984375
- ffn_gate: bfloat16 [2048, 2816], P('fs', 'tp'), may hold values from -0.125 to 0.125
- ffn_up: bfloat16 [2048, 2816], P('fs', 'tp'), may hold values from -0.125 to 0.125
- ffn_down: bfloat16 [2816, 2048], P('tp', 'fs'), may hold values from -0.109375 to 0.109375
- conv_value: bfloat16 [2048, 512], P('fs', 'tp'), may hold values from -0.125 to 0.125
- conv_gate: bfloat16 [2048, 512], P('fs', 'tp'), may hold values from -0.125 to 0.125
- depthwise: bfloat16 [31, 512], P(None, 'tp'), may hold values from -1.5 to 1.5
- conv_gain: bfloat16 [512], P('tp'), may hold values from 0.099609375 to 1.8984375
- conv_out: bfloat16 [512, 2048], P('tp', 'fs'), may hold values from -0.25 to 0.25
Outputs:
- mixed: bfloat16 [16, 512, 2048], P(('rep', 'fs'), 'tp')
All inputs are finite; a program needn't handle non-finite values.
Results may differ from a plain program's by a relative error of at most 0.0095.
Values may be sent and summed in bfloat16 or wider, within the bound.
A program may use at most 128 MiB of HBM per device.

v0:
```python
import functools

import jax
import jax.numpy as jnp
from jax import lax
from jax.experimental import pallas as pl
from jax.experimental.pallas import tpu as pltpu
from jax.sharding import PartitionSpec as P

ROW_EPS = 0.05
CHAN_EPS = 0.02
MESH = pl.DeviceIdType.MESH
LEAD = 1.5
LAG = 1.6


def rms_rows(stream, gain_vec):
    square_mean = jnp.mean(stream * stream, axis=-1, keepdims=True)
    return (stream * lax.rsqrt(square_mean + ROW_EPS) * gain_vec.astype(jnp.float32)).astype(
        jnp.bfloat16
    )


def swap(value):
    size = lax.axis_size("tp")
    return lax.ppermute(value, "tp", [(i, size - 1 - i) for i in range(size)])


def widen(normed):
    return jnp.concatenate([normed, swap(normed)])


def narrow(partial_value):
    rounded = partial_value.astype(jnp.bfloat16)
    half = rounded.shape[0] // 2
    return rounded[:half].astype(jnp.float32) + swap(rounded[half:]).astype(jnp.float32)


def reorder(rows):
    half = rows.shape[0] // 2
    flipped = jnp.concatenate([rows[half:], rows[:half]])
    return jnp.where(lax.axis_index("tp") == 0, rows, flipped)


def place():
    fs = lax.axis_index("fs")
    return lax.axis_index("rep"), lax.rem(fs, 2), fs // 2


class Gather:
    def __init__(self, depth, ins, slots, local_sems, recv_sems, send_sems):
        self.depth = depth
        self.ins, self.slots = ins, slots
        self.local_sems, self.recv_sems, self.send_sems = local_sems, recv_sems, send_sems
        self.x, self.y, self.z = place()

    def targets(self):
        other_x = {"rep": 1 - self.x}
        other_y = {"fs": self.z * 2 + 1 - self.y}
        up = {"fs": (self.z + 1) * 2 + self.y}
        down = {"fs": (self.z - 1) * 2 + self.y}
        return up, down, other_x, other_y

    def barrier(self):
        barrier = pltpu.get_barrier_semaphore()
        up, down, other_x, other_y = self.targets()
        has_up, has_down = self.z + 1 < self.depth, self.z > 0
        for target in (other_x, other_y):
            pl.semaphore_signal(barrier, inc=1, device_id=target, device_id_type=MESH)

        @pl.when(has_up)
        def _():
            pl.semaphore_signal(barrier, inc=1, device_id=up, device_id_type=MESH)

        @pl.when(has_down)
        def _():
            pl.semaphore_signal(barrier, inc=1, device_id=down, device_id_type=MESH)

        peers = 2 + has_up.astype(jnp.int32) + has_down.astype(jnp.int32)
        pl.semaphore_wait(barrier, peers)

    def local(self, m, c):
        k = self.z * 2 + self.y
        return pltpu.make_async_copy(
            self.ins[m].at[c], self.slots[m].at[k, c], self.local_sems[m].at[c]
        )

    def copy(self, m, c, k, way):
        piece = self.slots[m].at[k, c]
        return pltpu.make_async_remote_copy(
            src_ref=piece,
            dst_ref=piece,
            send_sem=self.send_sems[m].at[way, k, c],
            recv_sem=self.recv_sems[m].at[k, c],
            device_id=self.targets()[way],
            device_id_type=MESH,
        )

    def routes(self, m, c, side, d):
        x, y, z = self.x, self.y, self.z
        home = x == lax.rem(c, 2)
        has_up, has_down = z + 1 < self.depth, z > 0
        off = z < 0
        if side == "far_below":
            return (z - d) * 2 + 1 - y, z - d >= 0, (off, off, home, off)
        if side == "far_above":
            return (z + d) * 2 + 1 - y, z + d < self.depth, (off, off, home, off)
        if side == "own":
            return z * 2 + y, z >= 0, (has_up, has_down, off, home)
        if side == "below":
            return (z - d) * 2 + y, z - d >= 0, (has_up, off, off, home)
        return (z + d) * 2 + y, z + d < self.depth, (off, has_down, off, home)

    def event(self, m, side, d, finish=False):
        def step(c, carry):
            k, present, sends = self.routes(m, c, side, d)

            @pl.when(present)
            def _():
                if not finish:
                    if side == "own":
                        self.local(m, c).wait()
                    else:
                        self.copy(m, c, k, 2).wait_recv()
                for way, wanted in enumerate(sends):

                    @pl.when(wanted)
                    def _(way=way):
                        if finish:
                            self.copy(m, c, k, way).wait_send()
                        else:
                            self.copy(m, c, k, way).start()

            return carry

        lax.fori_loop(0, self.ins[m].shape[0], step, 0)

    def start_local(self):
        for m in range(len(self.ins)):

            def step(c, carry, m=m):
                self.local(m, c).start()
                return carry

            lax.fori_loop(0, self.ins[m].shape[0], step, 0)

    def plan(self):
        events = []
        span = self.depth - 1
        for m in range(len(self.ins)):
            start = m * span
            events.append((start - LEAD, m, "own", 0))
            events.append((start + LAG, m, "far_below", 0))
            for d in range(1, self.depth):
                events.append((start + d, m, "below", d))
                events.append((start + d, m, "above", d))
                events.append((start + d + LAG, m, "far_below", d))
                events.append((start + d + LAG, m, "far_above", d))
        return sorted(events, key=lambda event: event[0])

    def finish(self):
        for _, m, side, d in self.plan():
            self.event(m, side, d, finish=True)


def gather_kernel(depth, count, *refs):
    ins, slots = refs[:count], refs[count : 2 * count]
    sems = refs[2 * count :]
    gather = Gather(depth, ins, slots, sems[:count], sems[count : 2 * count], sems[2 * count :])
    gather.start_local()
    gather.barrier()
    for _, m, side, d in gather.plan():
        gather.event(m, side, d)
    gather.finish()


def gather_all(blocks):
    total = lax.axis_size("fs")
    count = len(blocks)
    outs = [jax.ShapeDtypeStruct((total, *b.shape), b.dtype) for b in blocks]
    dma = pltpu.SemaphoreType.DMA
    return pl.pallas_call(
        functools.partial(gather_kernel, total // 2, count),
        out_shape=outs,
        in_specs=[pl.BlockSpec(memory_space=pl.ANY)] * count,
        out_specs=[pl.BlockSpec(memory_space=pltpu.VMEM)] * count,
        scratch_shapes=[dma((b.shape[0],)) for b in blocks]
        + [dma((total, b.shape[0])) for b in blocks]
        + [dma((4, total, b.shape[0])) for b in blocks],
        compiler_params=pltpu.CompilerParams(
            collective_id=0, has_side_effects=True, vmem_limit_bytes=48 * 2**20
        ),
        name="gather_all",
    )(*blocks)


def hidden_units(gathered, whole_gate, whole_up):
    gate_rows = jnp.dot(gathered, whole_gate, preferred_element_type=jnp.float32)
    up_rows = jnp.dot(gathered, whole_up, preferred_element_type=jnp.float32)
    return (jax.nn.silu(gate_rows) * up_rows).astype(jnp.bfloat16)


def columns_of(blocks):
    return blocks.transpose(1, 0, 2).reshape(blocks.shape[1], -1)


def causal_taps(glu, kernel):
    length = glu.shape[0]
    taps = kernel.shape[0]
    padded = jnp.pad(glu, ((taps - 1, 0), (0, 0)))
    output = jnp.zeros_like(glu)
    for tap_index in range(taps):
        output = output + padded[tap_index : tap_index + length] * kernel[tap_index]
    return output


def chunked(block, pieces):
    return block.reshape(pieces, block.shape[0] // pieces, block.shape[1])


def shards(
    tokens,
    norm_first,
    norm_mixer,
    norm_second,
    ffn_gate,
    ffn_up,
    ffn_down,
    conv_value,
    conv_gate,
    depthwise,
    conv_gain,
    conv_out,
):
    width = tokens.shape[-1]
    stream = tokens.reshape(-1, width).astype(jnp.float32)
    first_rows = widen(rms_rows(stream, norm_first))
    small = jnp.concatenate([conv_value, conv_gate, conv_out.reshape(-1, conv_value.shape[1])])
    gate, up, down, small_all = gather_all(
        [chunked(ffn_gate, 4), chunked(ffn_up, 4), chunked(ffn_down, 4), chunked(small, 2)]
    )
    whole_gate = gate.reshape(-1, gate.shape[-1])
    whole_up = up.reshape(-1, up.shape[-1])
    whole_down = columns_of(down.reshape(down.shape[0], -1, down.shape[-1]))
    total = small_all.shape[0]
    small_all = small_all.reshape(total, -1, small_all.shape[-1])
    rows = conv_value.shape[0]
    channels_here = conv_value.shape[1]
    whole_value = small_all[:, :rows].reshape(-1, channels_here)
    whole_conv_gate = small_all[:, rows : 2 * rows].reshape(-1, channels_here)
    whole_out = columns_of(small_all[:, 2 * rows :].reshape(total, *conv_out.shape))

    hidden = hidden_units(first_rows, whole_gate, whole_up)
    stream = stream + 0.5 * narrow(jnp.dot(hidden, whole_down, preferred_element_type=jnp.float32))
    gathered = widen(rms_rows(stream, norm_mixer))
    values = jnp.dot(gathered, whole_value, preferred_element_type=jnp.float32)
    gates = jnp.dot(gathered, whole_conv_gate, preferred_element_type=jnp.float32)
    glu = reorder(values * jax.nn.sigmoid(gates))
    conv = causal_taps(glu, depthwise.astype(jnp.float32))
    channels = conv.shape[1] * lax.axis_size("tp")
    sums, squares = lax.psum((jnp.sum(conv, axis=1), jnp.sum(conv * conv, axis=1)), "tp")
    average = sums / channels
    spread = jnp.maximum(squares / channels - average * average, 0.0)
    centred = conv - average[:, None]
    activated = jax.nn.silu(
        centred * lax.rsqrt(spread[:, None] + CHAN_EPS) * conv_gain.astype(jnp.float32)
    ).astype(jnp.bfloat16)
    stream = stream + narrow(jnp.dot(reorder(activated), whole_out, preferred_element_type=jnp.float32))
    second_rows = widen(rms_rows(stream, norm_second))
    second_hidden = hidden_units(second_rows, whole_gate, whole_up)
    stream = stream + 0.5 * narrow(jnp.dot(second_hidden, whole_down, preferred_element_type=jnp.float32))
    return stream.astype(jnp.bfloat16).reshape(tokens.shape)


def solution(mesh):
    in_specs = (
        P(("rep", "fs"), "tp", None),
        P(),
        P(),
        P(),
        P("fs", "tp"),
        P("fs", "tp"),
        P("tp", "fs"),
        P("fs", "tp"),
        P("fs", "tp"),
        P(None, "tp"),
        P("tp"),
        P("tp", "fs"),
    )
    out_specs = P(("rep", "fs"), "tp", None)
    return jax.shard_map(shards, mesh=mesh, in_specs=in_specs, out_specs=out_specs, check_vma=False)
```

profile of v0, /device:TPU:0, one launch (start us, length us, event | category | flops | bytes accessed | tf_op | source)
XLA Modules:
  0.0 410.0 jit_solution(15881589800103331446)
XLA Ops:
  0.0 0.0 copy-start.2
  0.0 0.8 convert_element_type.73
  0.9 1.5 fusion
  2.4 2.5 fusion.2
  4.9 0.5 collective-permute-start
  5.4 0.0 copy-done.12
  5.4 0.0 copy-done.13
  5.4 0.0 copy-done.14
  5.4 0.0 copy-done
  5.4 0.0 copy-done.1
  5.5 0.0 copy-done.2
  5.5 319.2 %gather_all.1 = (bf16[8,4,64,1408]{3,2,1,0:T(8,128)(2,1)}, bf16[8,4,64,1408]{3,2,1,0:T(8,128)(2,1)}, bf16[8,4,352,256]{3,2,1,0:T(8,128)(2,1)}, bf16[8,2,384,256]{3,2,1,0:T(8,128)(2,1)S(1)}) custom-call(bf16[4,64,1408]{2,1,0:T(8,128)(2,1)S(1)} %bitcast.72, bf16[4,64,1408]{2,1,0:T(8,128)(2,1)S(1)} %bitcast.73, bf16[4,352,256]{2,1,0:T(8,128)(2,1)S(1)} %bitcast.74, ...), custom_call_target="tpu_custom_call" | custom-call | tf_op jit(solution)/shard_map/gather_all/pallas_call | solution.py:182
  324.6 8.3 %copy.13 = bf16[8,1408,256]{1,2,0:T(8,128)(2,1)} copy(bf16[8,1408,256]{2,1,0:T(8,128)(2,1)} %bitcast.77) | data formatting | bytes 11534336 | tf_op jit(solution)/shard_map/reshape | solution.py:244
  332.9 0.0 collective-permute-done
  332.9 8.3 %fusion.9 = f32[512,1408]{1,0:T(8,128)} fusion(bf16[2048,1408]{1,0:T(8,128)(2,1)} %bitcast.114, bf16[256,2048]{1,0:T(8,128)(2,1)} %collective-permute-done, bf16[256,2048]{1,0:T(8,128)(2,1)} %fusion.2), kind=kOutput, calls=%fused_computation.26 | convolution fusion | flops 2956984320 | bytes 10747904 | tf_op jit(solution)/shard_map/dot_general | solution.py:199
  341.2 14.0 %convolution_convert_fusion.2 = bf16[512,2048]{1,0:T(8,128)(2,1)} fusion(bf16[1408,2048]{0,1:T(8,128)(2,1)} %bitcast.75, f32[512,1408]{1,0:T(8,128)} %fusion.9, bf16[2048,1408]{1,0:T(8,128)(2,1)} %bitcast.112, bf16[256,2048]{1,0:T(8,128)(2,1)} %collective-permute-done, bf16[256,2048]{1,0:T(8,128)(2,1)} %fusion.2), kind=kOutput, calls=%fused_computation.5 | convolution fusion | flops 5915148288 | bytes 18612224 | tf_op jit(solution)/shard_map/dot_general | solution.py:254
  355.2 1.4 slice.298
  356.6 0.0 copy-start.7
  356.6 0.1 collective-permute-start.1
  356.7 0.0 copy-done.16
  356.7 2.6 collective-permute-done.1
  359.3 0.0 copy-done.3
  359.3 2.2 multiply_reduce_fusion.1
  361.6 0.0 copy-done.7
  361.6 1.7 multiply_convert_fusion.3
  363.3 0.0 copy-done.5
  363.3 0.1 collective-permute-start.2
  363.4 1.8 fusion.65
  365.2 1.7 copy.15
  367.0 0.0 copy-done.19
  367.0 0.0 copy-done.15
  367.1 0.0 collective-permute-done.2
  367.1 0.0 copy-done.11
  367.1 0.0 copy-start.10
  367.1 2.4 fusion.15
  369.5 0.0 copy-done.10
  369.5 2.3 fusion.11
  371.8 0.1 maximum_select_fusion
  371.9 2.4 fusion.64
  374.2 2.5 all-reduce.1
  376.8 0.2 multiply_convert_fusion.6
  377.0 0.0 copy-start.17
  377.0 0.0 copy-start.4
  377.1 0.0 copy-start.6
  377.1 0.0 copy-start.8
  377.1 0.8 convolution_convert_fusion
  377.8 0.1 slice.338
  377.9 0.4 collective-permute-start.3
  378.3 0.0 copy-done.17
  378.3 2.3 collective-permute-done.3
  380.6 0.0 copy-done.4
  380.6 0.0 copy-done.6
  380.7 1.0 multiply_reduce_fusion
  381.7 0.3 multiply_convert_fusion.2
  381.9 0.4 collective-permute-start.4
  382.3 2.3 collective-permute-done.4
  384.7 1.0 copy-done.18
  385.6 0.0 slice-done
  385.6 5.1 %fusion.5 = f32[512,1408]{1,0:T(8,128)} fusion(bf16[2048,1408]{1,0:T(8,128)(2,1)S(1)} %bitcast.117, bf16[256,2048]{1,0:T(8,128)(2,1)S(1)} %collective-permute-done.4, bf16[256,2048]{1,0:T(8,128)(2,1)S(1)} %multiply_convert_fusion.2), kind=kOutput, calls=%fused_computation.22 | convolution fusion | flops 2956984320 | bytes 10747904 | tf_op jit(solution)/shard_map/dot_general | solution.py:199
  390.7 13.7 %convolution_convert_fusion.1 = bf16[512,2048]{1,0:T(8,128)(2,1)} fusion(bf16[1408,2048]{0,1:T(8,128)(2,1)} %bitcast.76, f32[512,1408]{1,0:T(8,128)} %fusion.5, bf16[2048,1408]{1,0:T(8,128)(2,1)} %bitcast.113, bf16[256,2048]{1,0:T(8,128)(2,1)} %copy-done.18, bf16[256,2048]{1,0:T(8,128)(2,1)S(1)} %multiply_convert_fusion.2), kind=kOutput, calls=%fused_computation.4 | convolution fusion | flops 5915148288 | bytes 18612224 | tf_op jit(solution)/shard_map/dot_general | solution.py:271
  404.3 1.4 slice.340
  405.8 0.4 collective-permute-start.5
  406.2 2.3 collective-permute-done.5
  408.5 1.5 fusion.16
  (31 shorter events, 0.2 us)
Async XLA Ops:
  0.0 5.4 %copy-start.12 = (bf16[256,256]{1,0:T(8,128)(2,1)S(1)}, bf16[256,256]{1,0:T(8,128)(2,1)}, u32[]{:S(2)}) copy-start(bf16[256,256]{1,0:T(8,128)(2,1)} %param.23) | copy-start | bytes 393220
  0.0 5.4 %copy-start.13 = (bf16[256,256]{1,0:T(8,128)(2,1)S(1)}, bf16[256,256]{1,0:T(8,128)(2,1)}, u32[]{:S(2)}) copy-start(bf16[256,256]{1,0:T(8,128)(2,1)} %param.20) | copy-start | bytes 393220
  0.0 5.4 %copy-start.14 = (bf16[256,256]{1,0:T(8,128)(2,1)S(1)}, bf16[256,256]{1,0:T(8,128)(2,1)}, u32[]{:S(2)}) copy-start(bf16[256,256]{1,0:T(8,128)(2,1)} %param.19) | copy-start | bytes 393220
  0.0 5.4 %copy-start = (bf16[256,1408]{1,0:T(8,128)(2,1)S(1)}, bf16[256,1408]{1,0:T(8,128)(2,1)}, u32[]{:S(2)}) copy-start(bf16[256,1408]{1,0:T(8,128)(2,1)} %param.16) | copy-start | bytes 2162692
  0.0 5.4 %copy-start.1 = (bf16[256,1408]{1,0:T(8,128)(2,1)S(1)}, bf16[256,1408]{1,0:T(8,128)(2,1)}, u32[]{:S(2)}) copy-start(bf16[256,1408]{1,0:T(8,128)(2,1)} %param.17) | copy-start | bytes 2162692
  0.0 5.4 %copy-start.2 = (bf16[1408,256]{1,0:T(8,128)(2,1)S(1)}, bf16[1408,256]{1,0:T(8,128)(2,1)}, u32[]{:S(2)}) copy-start(bf16[1408,256]{1,0:T(8,128)(2,1)} %param.18) | copy-start | bytes 2162692
  4.9 328.0 %collective-permute-start = (bf16[256,2048]{1,0:T(8,128)(2,1)}, bf16[256,2048]{1,0:T(8,128)(2,1)}, u32[]{:S(2)}, u32[]{:S(2)}) collective-permute-start(bf16[256,2048]{1,0:T(8,128)(2,1)} %fusion.2), channel_id=1, source_target_pairs={{0,1},{1,0},{2,3},{3,2},{4,5},{5,4},{6,7},{7,6},{8,9},{9,8},{10,11... | collective-permute-start | bytes 3145736 | tf_op jit(solution)/shard_map/ppermute | solution.py:26
  355.2 1.5 copy-start.16
  355.2 4.1 %copy-start.3 = (bf16[1,256,2048]{2,1,0:T(8,128)(2,1)S(1)}, bf16[1,256,2048]{2,1,0:T(8,128)(2,1)}, u32[]{:S(2)}) copy-start(bf16[1,256,2048]{2,1,0:T(8,128)(2,1)} %param.12) | copy-start | bytes 3145732
  356.6 5.0 %copy-start.7 = (bf16[512,2048]{1,0:T(8,128)(2,1)S(1)}, bf16[512,2048]{1,0:T(8,128)(2,1)}, u32[]{:S(2)}) copy-start(bf16[512,2048]{1,0:T(8,128)(2,1)} %convolution_convert_fusion.2) | copy-start | bytes 6291460
  356.6 2.7 collective-permute-start.1
  359.3 3.9 copy-start.5
  363.3 3.8 collective-permute-start.2
  365.2 1.8 copy-start.19
  365.2 1.8 copy-start.15
  365.2 1.9 copy-start.11
  367.1 2.4 copy-start.10
  377.0 1.3 copy-start.17
  377.0 3.6 copy-start.4
  377.1 3.6 copy-start.6
  377.1 3.6 copy-start.8
  377.9 2.7 collective-permute-start.3
  378.3 7.3 %slice-start = ((s8[5767168]{0:T(1024)(128)(4,1)}), s8[4194304]{0:T(1024)(128)(4,1)S(1)}, s32[]{:S(2)}) async-start(s8[5767168]{0:T(1024)(128)(4,1)} %bitcast.115), calls=%async_computation | async-start | bytes 8388608
  378.3 7.3 %slice-start.1 = ((s8[5767168]{0:T(1024)(128)(4,1)}), s8[1572864]{0:T(1024)(128)(4,1)S(1)}, s32[]{:S(2)}) async-start(s8[5767168]{0:T(1024)(128)(4,1)} %bitcast.115), calls=%async_computation.1 | async-start | bytes 3145728
  381.9 2.7 collective-permute-start.4
  384.6 1.0 copy-start.18
  404.3 4.2 %copy-start.9 = (bf16[512,2048]{1,0:T(8,128)(2,1)S(1)}, bf16[512,2048]{1,0:T(8,128)(2,1)}, u32[]{:S(2)}) copy-start(bf16[512,2048]{1,0:T(8,128)(2,1)} %convolution_convert_fusion.1) | copy-start | bytes 6291460
  405.8 2.7 collective-permute-start.5
where the time goes:
time: 411 us; the launch traced here: 410 us
  Pallas kernels  319 us (78%)
  matrix products  46.3 us (11%)
  local copies, waits for them, and re-layouts  15.9 us (4%)
  other arithmetic  14.3 us (3%)
  waiting for transfers between devices  9.58 us (2%)
    pallas_call x1, Pallas kernels, gather_all(): pl.pallas_call(functools.partial(gather_kernel, total // 2, count), out_s...  319 us
    dot_general x1, matrix products, shards(): jnp.dot(hidden, whole_down, preferred_element_type=jnp.float32)  14 us
    dot_general x1, matrix products, shards(): jnp.dot(second_hidden, whole_down, preferred_element_type=jnp.float32)  13.7 us
    dot_general x2, matrix products, hidden_units(): up_rows = jnp.dot(gathered, whole_up, preferred_element_type=jnp.float32)  13.3 us
    ppermute x6, waiting for transfers between devices, swap(): return lax.ppermute(value, 'tp', [(i, size - 1 - i) for i in range(size)])  9.58 us
    reshape x1, local copies, waits for them, and re-layouts, shards(): whole_down = columns_of(down.reshape(down.shape[0], -1, down.shape[-1]))  8.26 us
  transfers between devices with their start and end apart: 6, of which 4 were waited for; matrix products, arithmetic and copies ran while one was open for 3% of the time, Pallas kernels for 78%

commit v1 on v0

v1 whole, which is shorter than its diff:
```python
import functools

import jax
import jax.numpy as jnp
from jax import lax
from jax.experimental import pallas as pl
from jax.experimental.pallas import tpu as pltpu
from jax.sharding import PartitionSpec as P

ROW_EPS = 0.05
CHAN_EPS = 0.02
MESH = pl.DeviceIdType.MESH
CHUNKS = 8
SHARES = ((6, 5), (6, 4), (6, 5), (6, 5))
UP, DOWN, OVER_X, OVER_Y = range(4)


def rms_rows(stream, gain_vec):
    square_mean = jnp.mean(stream * stream, axis=-1, keepdims=True)
    return (stream * lax.rsqrt(square_mean + ROW_EPS) * gain_vec.astype(jnp.float32)).astype(
        jnp.bfloat16
    )


def swap(value):
    size = lax.axis_size("tp")
    return lax.ppermute(value, "tp", [(i, size - 1 - i) for i in range(size)])


def widen(normed):
    return jnp.concatenate([normed, swap(normed)])


def narrow(partial_value):
    rounded = partial_value.astype(jnp.bfloat16)
    half = rounded.shape[0] // 2
    return rounded[:half].astype(jnp.float32) + swap(rounded[half:]).astype(jnp.float32)


def reorder(rows):
    half = rows.shape[0] // 2
    flipped = jnp.concatenate([rows[half:], rows[:half]])
    return jnp.where(lax.axis_index("tp") == 0, rows, flipped)


def place():
    fs = lax.axis_index("fs")
    return lax.axis_index("rep"), lax.rem(fs, 2), fs // 2


class Gather:
    def __init__(self, depth, shares, ins, slots, local_sems, recv_sems, side_sems, send_sems):
        self.depth, self.shares = depth, shares
        self.ins, self.slots = ins, slots
        self.local_sems, self.recv_sems = local_sems, recv_sems
        self.side_sems, self.send_sems = side_sems, send_sems
        self.x, self.y, self.z = place()
        self.has_up, self.has_down = self.z + 1 < depth, self.z > 0
        self.own = self.z * 2 + self.y

    def target(self, way):
        if way == UP:
            return {"fs": (self.z + 1) * 2 + self.y}
        if way == DOWN:
            return {"fs": (self.z - 1) * 2 + self.y}
        if way == OVER_X:
            return {"rep": 1 - self.x}
        return {"fs": self.z * 2 + 1 - self.y}

    def barrier(self):
        barrier = pltpu.get_barrier_semaphore()
        for way in (OVER_X, OVER_Y):
            pl.semaphore_signal(barrier, inc=1, device_id=self.target(way), device_id_type=MESH)
        for way, present in ((UP, self.has_up), (DOWN, self.has_down)):

            @pl.when(present)
            def _(way=way):
                pl.semaphore_signal(barrier, inc=1, device_id=self.target(way), device_id_type=MESH)

        peers = 2 + self.has_up.astype(jnp.int32) + self.has_down.astype(jnp.int32)
        pl.semaphore_wait(barrier, peers)

    def count(self, m):
        return self.slots[m].shape[1]

    def chunk(self, m, e, mine=True):
        count = self.count(m)
        flip = self.x if mine else 1 - self.x
        return e + flip * (count - 1 - 2 * e)

    def chunks(self, m, first, last, mine=True):
        count = self.count(m)
        flip = self.x if mine else 1 - self.x
        return pl.ds(first + flip * (count - last - first), last - first)

    def local(self, m):
        return pltpu.make_async_copy(self.ins[m], self.slots[m].at[self.own], self.local_sems.at[m])

    def copy(self, m, k, c, way):
        piece = self.slots[m].at[k, c]
        recv_sem = self.side_sems[m].at[k] if way == OVER_X else self.recv_sems[m].at[k, c]
        return pltpu.make_async_remote_copy(
            src_ref=piece,
            dst_ref=piece,
            send_sem=self.send_sems[m].at[way, k],
            recv_sem=recv_sem,
            device_id=self.target(way),
            device_id_type=MESH,
        )

    def spread(self, m, k, e, ways):
        c = self.chunk(m, e)
        for way, wanted in ways:
            if wanted is True:
                self.copy(m, k, c, way).start()
            elif wanted is not False:
                pl.when(wanted)(lambda way=way: self.copy(m, k, c, way).start())

    def start_local(self):
        for m in range(len(self.ins)):
            self.local(m).start()

    def start_own(self, m):
        along, across = self.shares[m]
        self.local(m).wait()
        for e in range(along):
            self.spread(m, self.own, e, ((UP, self.has_up), (DOWN, self.has_down), (OVER_Y, e < across)))

    def pieces(self, d):
        return ((self.z - d, self.z - d >= 0, self.has_up, UP), (self.z + d, self.z + d < self.depth, self.has_down, DOWN))

    def arrive_along(self, m, d, e):
        along, across = self.shares[m]
        spare = self.count(m) - along
        for at, present, further, way in self.pieces(d):

            @pl.when(present)
            def _(at=at, further=further, way=way):
                k = at * 2 + self.y
                self.copy(m, k, self.chunk(m, e), UP).wait_recv()
                self.spread(m, k, e, ((way, further), (OVER_Y, e < across), (OVER_X, e < spare)))

    def arrive_across(self, m, d, e):
        spare = self.count(m) - self.shares[m][1]
        for side, (at, present, _, _) in enumerate(self.pieces(d)):
            if side == 1:
                present = jnp.logical_and(present, d > 0)

            @pl.when(present)
            def _(at=at):
                k = at * 2 + 1 - self.y
                self.copy(m, k, self.chunk(m, e), OVER_Y).wait_recv()
                self.spread(m, k, e, ((OVER_X, e < spare),))

    def run(self):
        total = len(self.ins)
        self.start_own(0)
        for m in range(total):
            along, across = self.shares[m]

            def step(r, carry, m=m, along=along, across=across):
                if m + 1 < total:

                    @pl.when(r == max(self.depth - 2, 0))
                    def _():
                        self.start_own(m + 1)

                for e in range(max(along, across)):
                    if e < along:
                        self.arrive_along(m, r + 1, e)
                    if e < across:
                        self.arrive_across(m, r, e)
                return carry

            lax.fori_loop(0, self.depth, step, 0)

    def side(self, m, k, first, last, mine):
        piece = self.slots[m].at[k, self.chunks(m, first, last, mine)]
        return pltpu.make_async_remote_copy(
            src_ref=piece,
            dst_ref=piece,
            send_sem=self.send_sems[m].at[OVER_X, k],
            recv_sem=self.side_sems[m].at[k],
            device_id=self.target(OVER_X),
            device_id_type=MESH,
        )

    def sent(self, m, k, last, way):
        piece = self.slots[m].at[k, self.chunks(m, 0, last)]
        return pltpu.make_async_remote_copy(
            src_ref=piece,
            dst_ref=piece,
            send_sem=self.send_sems[m].at[way, k],
            recv_sem=self.side_sems[m].at[k],
            device_id=self.target(way),
            device_id_type=MESH,
        )

    def drain(self):
        for m in range(len(self.ins)):
            along, across = self.shares[m]
            count = self.count(m)

            def step(d, carry, m=m, along=along, across=across, count=count):
                for side, (at, present, further, way) in enumerate(self.pieces(d)):
                    if side == 1:
                        present = jnp.logical_and(present, d > 0)

                    @pl.when(present)
                    def _(at=at, further=further, way=way):
                        k, cross = at * 2 + self.y, at * 2 + 1 - self.y

                        @pl.when(d > 0)
                        def _():
                            self.side(m, k, 0, count - along, False).wait_recv()
                            self.side(m, k, 0, count - along, True).wait_send()

                        self.side(m, cross, 0, count - across, False).wait_recv()
                        self.side(m, cross, 0, count - across, True).wait_send()
                        self.sent(m, k, across, OVER_Y).wait_send()
                        pl.when(further)(lambda: self.sent(m, k, along, way).wait_send())

                return carry

            lax.fori_loop(0, self.depth, step, 0)

            @pl.when(self.has_down)
            def _(m=m, along=along):
                self.sent(m, self.own, along, DOWN).wait_send()


def gather_kernel(depth, shares, count, *refs):
    ins, slots = refs[:count], refs[count : 2 * count]
    sems = refs[2 * count :]
    local_sems, sems = sems[0], sems[1:]
    gather = Gather(depth, shares, ins, slots, local_sems, sems[:count], sems[count : 2 * count], sems[2 * count :])
    gather.start_local()
    gather.barrier()
    gather.run()
    gather.drain()


def gather_all(blocks, shares):
    total = lax.axis_size("fs")
    count = len(blocks)
    outs = [jax.ShapeDtypeStruct((total, *b.shape), b.dtype) for b in blocks]
    dma = pltpu.SemaphoreType.DMA
    return pl.pallas_call(
        functools.partial(gather_kernel, total // 2, shares, count),
        out_shape=outs,
        in_specs=[pl.BlockSpec(memory_space=pl.ANY)] * count,
        out_specs=[pl.BlockSpec(memory_space=pltpu.VMEM)] * count,
        scratch_shapes=[dma((count,))]
        + [dma((total, b.shape[0])) for b in blocks]
        + [dma((total,)) for b in blocks]
        + [dma((4, total)) for b in blocks],
        compiler_params=pltpu.CompilerParams(
            collective_id=0, has_side_effects=True, vmem_limit_bytes=48 * 2**20
        ),
        name="gather_all",
    )(*blocks)


def hidden_units(gathered, whole_gate, whole_up):
    gate_rows = jnp.dot(gathered, whole_gate, preferred_element_type=jnp.float32)
    up_rows = jnp.dot(gathered, whole_up, preferred_element_type=jnp.float32)
    return (jax.nn.silu(gate_rows) * up_rows).astype(jnp.bfloat16)


def columns_of(blocks):
    return blocks.transpose(1, 0, 2).reshape(blocks.shape[1], -1)


def causal_taps(glu, kernel):
    length = glu.shape[0]
    taps = kernel.shape[0]
    padded = jnp.pad(glu, ((taps - 1, 0), (0, 0)))
    output = jnp.zeros_like(glu)
    for tap_index in range(taps):
        output = output + padded[tap_index : tap_index + length] * kernel[tap_index]
    return output


def chunked(block, pieces):
    return block.reshape(pieces, block.shape[0] // pieces, block.shape[1])


def shards(
    tokens,
    norm_first,
    norm_mixer,
    norm_second,
    ffn_gate,
    ffn_up,
    ffn_down,
    conv_value,
    conv_gate,
    depthwise,
    conv_gain,
    conv_out,
):
    width = tokens.shape[-1]
    stream = tokens.reshape(-1, width).astype(jnp.float32)
    first_rows = widen(rms_rows(stream, norm_first))
    small = jnp.concatenate([conv_value, conv_gate, conv_out.reshape(-1, conv_value.shape[1])])
    gate, up, down, small_all = gather_all(
        [chunked(block, CHUNKS) for block in (ffn_gate, ffn_up, ffn_down, small)], SHARES
    )
    whole_gate = gate.reshape(-1, gate.shape[-1])
    whole_up = up.reshape(-1, up.shape[-1])
    whole_down = columns_of(down.reshape(down.shape[0], -1, down.shape[-1]))
    total = small_all.shape[0]
    small_all = small_all.reshape(total, -1, small_all.shape[-1])
    rows = conv_value.shape[0]
    channels_here = conv_value.shape[1]
    whole_value = small_all[:, :rows].reshape(-1, channels_here)
    whole_conv_gate = small_all[:, rows : 2 * rows].reshape(-1, channels_here)
    whole_out = columns_of(small_all[:, 2 * rows :].reshape(total, *conv_out.shape))

    hidden = hidden_units(first_rows, whole_gate, whole_up)
    stream = stream + 0.5 * narrow(jnp.dot(hidden, whole_down, preferred_element_type=jnp.float32))
    gathered = widen(rms_rows(stream, norm_mixer))
    values = jnp.dot(gathered, whole_value, preferred_element_type=jnp.float32)
    gates = jnp.dot(gathered, whole_conv_gate, preferred_element_type=jnp.float32)
    glu = reorder(values * jax.nn.sigmoid(gates))
    conv = causal_taps(glu, depthwise.astype(jnp.float32))
    channels = conv.shape[1] * lax.axis_size("tp")
    sums, squares = lax.psum((jnp.sum(conv, axis=1), jnp.sum(conv * conv, axis=1)), "tp")
    average = sums / channels
    spread = jnp.maximum(squares / channels - average * average, 0.0)
    centred = conv - average[:, None]
    activated = jax.nn.silu(
        centred * lax.rsqrt(spread[:, None] + CHAN_EPS) * conv_gain.astype(jnp.float32)
    ).astype(jnp.bfloat16)
    stream = stream + narrow(jnp.dot(reorder(activated), whole_out, preferred_element_type=jnp.float32))
    second_rows = widen(rms_rows(stream, norm_second))
    second_hidden = hidden_units(second_rows, whole_gate, whole_up)
    stream = stream + 0.5 * narrow(jnp.dot(second_hidden, whole_down, preferred_element_type=jnp.float32))
    return stream.astype(jnp.bfloat16).reshape(tokens.shape)


def solution(mesh):
    in_specs = (
        P(("rep", "fs"), "tp", None),
        P(),
        P(),
        P(),
        P("fs", "tp"),
        P("fs", "tp"),
        P("tp", "fs"),
        P("fs", "tp"),
        P("fs", "tp"),
        P(None, "tp"),
        P("tp"),
        P("tp", "fs"),
    )
    out_specs = P(("rep", "fs"), "tp", None)
    return jax.shard_map(shards, mesh=mesh, in_specs=in_specs, out_specs=out_specs, check_vma=False)
```

time: 411 us -> 252 us (0.61)
  Pallas kernels: 319 us -> 161 us
    pallas_call x1, Pallas kernels: 319 us -> 161 us  [gather_all(): pl.pallas_call(functools.partial(gather_kernel, total // 2, shares, count...]
  transfers between devices with their start and end apart: 6 -> 6, of which waited for: 4 -> 4; matrix products, arithmetic and copies ran while one was open for 3% -> 5% of each run, Pallas kernels for 78% -> 64%
where the time goes in v1:
time: 252 us; the launch traced here: 251 us
  Pallas kernels  161 us (64%)
  matrix products  46.3 us (18%)
  local copies, waits for them, and re-layouts  15.9 us (6%)
  other arithmetic  14.3 us (6%)
  waiting for transfers between devices  9.56 us (4%)
    pallas_call x1, Pallas kernels, gather_all(): pl.pallas_call(functools.partial(gather_kernel, total // 2, shares, count...  161 us
    dot_general x1, matrix products, shards(): jnp.dot(hidden, whole_down, preferred_element_type=jnp.float32)  14 us
    dot_general x1, matrix products, shards(): jnp.dot(second_hidden, whole_down, preferred_element_type=jnp.float32)  13.6 us
    dot_general x2, matrix products, hidden_units(): up_rows = jnp.dot(gathered, whole_up, preferred_element_type=jnp.float32)  13.3 us
    ppermute x6, waiting for transfers between devices, swap(): return lax.ppermute(value, 'tp', [(i, size - 1 - i) for i in range(size)])  9.56 us
    reshape x1, local copies, waits for them, and re-layouts, shards(): whole_down = columns_of(down.reshape(down.shape[0], -1, down.shape[-1]))  8.26 us
  transfers between devices with their start and end apart: 6, of which 4 were waited for; matrix products, arithmetic and copies ran while one was open for 5% of the time, Pallas kernels for 64%

profile of v1, /device:TPU:0, one launch (start us, length us, event | category | flops | bytes accessed | tf_op | source)
XLA Modules:
  0.0 251.4 jit_solution(13397332338904865030)
XLA Ops:
  0.0 0.0 copy-start.2
  0.0 0.8 convert_element_type.73
  0.9 1.5 fusion
  2.4 2.5 fusion.2
  4.9 0.5 collective-permute-start
  5.4 0.0 copy-done.12
  5.4 0.0 copy-done.13
  5.4 0.0 copy-done.14
  5.4 0.0 copy-done
  5.4 0.0 copy-done.1
  5.5 0.0 copy-done.2
  5.5 160.6 %gather_all.1 = (bf16[8,8,32,1408]{3,2,1,0:T(8,128)(2,1)}, bf16[8,8,32,1408]{3,2,1,0:T(8,128)(2,1)}, bf16[8,8,176,256]{3,2,1,0:T(8,128)(2,1)}, bf16[8,8,96,256]{3,2,1,0:T(8,128)(2,1)S(1)}) custom-call(bf16[8,32,1408]{2,1,0:T(8,128)(2,1)S(1)} %bitcast.72, bf16[8,32,1408]{2,1,0:T(8,128)(2,1)S(1)} %bitcast.73, bf16[8,176,256]{2,1,0:T(8,128)(2,1)S(1)} %bitcast.74, ...), custom_call_target="tpu_custom_call" | custom-call | tf_op jit(solution)/shard_map/gather_all/pallas_call | solution.py:248
  166.1 8.3 %copy.13 = bf16[8,1408,256]{1,2,0:T(8,128)(2,1)} copy(bf16[8,1408,256]{2,1,0:T(8,128)(2,1)} %bitcast.77) | data formatting | bytes 11534336 | tf_op jit(solution)/shard_map/reshape | solution.py:311
  174.3 0.0 collective-permute-done
  174.3 8.3 %fusion.9 = f32[512,1408]{1,0:T(8,128)} fusion(bf16[2048,1408]{1,0:T(8,128)(2,1)} %bitcast.114, bf16[256,2048]{1,0:T(8,128)(2,1)} %collective-permute-done, bf16[256,2048]{1,0:T(8,128)(2,1)} %fusion.2), kind=kOutput, calls=%fused_computation.26 | convolution fusion | flops 2956984320 | bytes 10747904 | tf_op jit(solution)/shard_map/dot_general | solution.py:266
  182.6 14.0 %convolution_convert_fusion.2 = bf16[512,2048]{1,0:T(8,128)(2,1)} fusion(bf16[1408,2048]{0,1:T(8,128)(2,1)} %bitcast.75, f32[512,1408]{1,0:T(8,128)} %fusion.9, bf16[2048,1408]{1,0:T(8,128)(2,1)} %bitcast.112, bf16[256,2048]{1,0:T(8,128)(2,1)} %collective-permute-done, bf16[256,2048]{1,0:T(8,128)(2,1)} %fusion.2), kind=kOutput, calls=%fused_computation.5 | convolution fusion | flops 5915148288 | bytes 18612224 | tf_op jit(solution)/shard_map/dot_general | solution.py:321
  196.6 1.4 slice.298
  198.0 0.0 copy-start.7
  198.0 0.1 collective-permute-start.1
  198.1 0.0 copy-done.16
  198.1 2.6 %collective-permute-done.1 = bf16[256,2048]{1,0:T(8,128)(2,1)S(1)} collective-permute-done((bf16[256,2048]{1,0:T(8,128)(2,1)S(1)}, bf16[256,2048]{1,0:T(8,128)(2,1)S(1)}, u32[]{:S(2)}, u32[]{:S(2)}) %collective-permute-start.1) | collective-permute-done | bytes 1048608 | tf_op jit(solution)/shard_map/ppermute | solution.py:27
  200.7 0.0 copy-done.3
  200.7 2.2 multiply_reduce_fusion.1
  203.0 0.0 copy-done.7
  203.0 1.7 multiply_convert_fusion.3
  204.7 0.0 copy-done.5
  204.7 0.1 collective-permute-start.2
  204.8 1.8 fusion.65
  206.6 1.7 copy.15
  208.4 0.0 copy-done.19
  208.4 0.0 copy-done.15
  208.5 0.0 collective-permute-done.2
  208.5 0.0 copy-done.11
  208.5 0.0 copy-start.10
  208.5 2.4 fusion.15
  210.9 0.0 copy-done.10
  210.9 2.3 fusion.11
  213.2 0.1 maximum_select_fusion
  213.3 2.4 fusion.64
  215.7 2.5 all-reduce.1
  218.2 0.2 multiply_convert_fusion.6
  218.5 0.0 copy-start.17
  218.5 0.0 copy-start.4
  218.5 0.0 copy-start.6
  218.5 0.0 copy-start.8
  218.5 0.8 convolution_convert_fusion
  219.3 0.1 slice.338
  219.3 0.4 collective-permute-start.3
  219.8 0.0 copy-done.17
  219.8 2.3 collective-permute-done.3
  222.1 0.0 copy-done.4
  222.1 1.0 multiply_reduce_fusion
  223.1 0.3 multiply_convert_fusion.2
  223.3 0.4 collective-permute-start.4
  223.8 2.3 collective-permute-done.4
  226.1 1.0 copy-done.18
  227.0 0.0 slice-done
  227.0 5.1 %fusion.5 = f32[512,1408]{1,0:T(8,128)} fusion(bf16[2048,1408]{1,0:T(8,128)(2,1)S(1)} %bitcast.117, bf16[256,2048]{1,0:T(8,128)(2,1)S(1)} %collective-permute-done.4, bf16[256,2048]{1,0:T(8,128)(2,1)S(1)} %multiply_convert_fusion.2), kind=kOutput, calls=%fused_computation.22 | convolution fusion | flops 2956984320 | bytes 10747904 | tf_op jit(solution)/shard_map/dot_general | solution.py:266
  232.1 13.6 %convolution_convert_fusion.1 = bf16[512,2048]{1,0:T(8,128)(2,1)} fusion(bf16[1408,2048]{0,1:T(8,128)(2,1)} %bitcast.76, f32[512,1408]{1,0:T(8,128)} %fusion.5, bf16[2048,1408]{1,0:T(8,128)(2,1)} %bitcast.113, bf16[256,2048]{1,0:T(8,128)(2,1)} %copy-done.18, bf16[256,2048]{1,0:T(8,128)(2,1)S(1)} %multiply_convert_fusion.2), kind=kOutput, calls=%fused_computation.4 | convolution fusion | flops 5915148288 | bytes 18612224 | tf_op jit(solution)/shard_map/dot_general | solution.py:338
  245.8 1.4 slice.340
  247.2 0.4 collective-permute-start.5
  247.6 2.3 collective-permute-done.5
  249.9 0.0 copy-done.9
  249.9 1.5 fusion.16
  (31 shorter events, 0.2 us)
Async XLA Ops:
  0.0 5.4 %copy-start.12 = (bf16[256,256]{1,0:T(8,128)(2,1)S(1)}, bf16[256,256]{1,0:T(8,128)(2,1)}, u32[]{:S(2)}) copy-start(bf16[256,256]{1,0:T(8,128)(2,1)} %param.23) | copy-start | bytes 393220
  0.0 5.4 %copy-start.13 = (bf16[256,256]{1,0:T(8,128)(2,1)S(1)}, bf16[256,256]{1,0:T(8,128)(2,1)}, u32[]{:S(2)}) copy-start(bf16[256,256]{1,0:T(8,128)(2,1)} %param.20) | copy-start | bytes 393220
  0.0 5.4 %copy-start.14 = (bf16[256,256]{1,0:T(8,128)(2,1)S(1)}, bf16[256,256]{1,0:T(8,128)(2,1)}, u32[]{:S(2)}) copy-start(bf16[256,256]{1,0:T(8,128)(2,1)} %param.19) | copy-start | bytes 393220
  0.0 5.4 %copy-start = (bf16[256,1408]{1,0:T(8,128)(2,1)S(1)}, bf16[256,1408]{1,0:T(8,128)(2,1)}, u32[]{:S(2)}) copy-start(bf16[256,1408]{1,0:T(8,128)(2,1)} %param.16) | copy-start | bytes 2162692
  0.0 5.4 %copy-start.1 = (bf16[256,1408]{1,0:T(8,128)(2,1)S(1)}, bf16[256,1408]{1,0:T(8,128)(2,1)}, u32[]{:S(2)}) copy-start(bf16[256,1408]{1,0:T(8,128)(2,1)} %param.17) | copy-start | bytes 2162692
  0.0 5.4 %copy-start.2 = (bf16[1408,256]{1,0:T(8,128)(2,1)S(1)}, bf16[1408,256]{1,0:T(8,128)(2,1)}, u32[]{:S(2)}) copy-start(bf16[1408,256]{1,0:T(8,128)(2,1)} %param.18) | copy-start | bytes 2162692
  4.9 169.4 %collective-permute-start = (bf16[256,2048]{1,0:T(8,128)(2,1)}, bf16[256,2048]{1,0:T(8,128)(2,1)}, u32[]{:S(2)}, u32[]{:S(2)}) collective-permute-start(bf16[256,2048]{1,0:T(8,128)(2,1)} %fusion.2), channel_id=1, source_target_pairs={{0,1},{1,0},{2,3},{3,2},{4,5},{5,4},{6,7},{7,6},{8,9},{9,8},{10,11... | collective-permute-start | bytes 3145736 | tf_op jit(solution)/shard_map/ppermute | solution.py:27
  196.6 1.5 copy-start.16
  196.6 4.1 %copy-start.3 = (bf16[1,256,2048]{2,1,0:T(8,128)(2,1)S(1)}, bf16[1,256,2048]{2,1,0:T(8,128)(2,1)}, u32[]{:S(2)}) copy-start(bf16[1,256,2048]{2,1,0:T(8,128)(2,1)} %param.12) | copy-start | bytes 3145732
  198.0 5.0 %copy-start.7 = (bf16[512,2048]{1,0:T(8,128)(2,1)S(1)}, bf16[512,2048]{1,0:T(8,128)(2,1)}, u32[]{:S(2)}) copy-start(bf16[512,2048]{1,0:T(8,128)(2,1)} %convolution_convert_fusion.2) | copy-start | bytes 6291460
  198.0 2.7 %collective-permute-start.1 = (bf16[256,2048]{1,0:T(8,128)(2,1)S(1)}, bf16[256,2048]{1,0:T(8,128)(2,1)S(1)}, u32[]{:S(2)}, u32[]{:S(2)}) collective-permute-start(bf16[256,2048]{1,0:T(8,128)(2,1)S(1)} %slice.298), channel_id=1, source_target_pairs={{0,1},{1,0},{2,3},{3,2},{4,5},{5,4},{6,7},{7,6},{8,9},{9,8},{10,11... | collective-permute-start | bytes 3145736 | tf_op jit(solution)/shard_map/ppermute | solution.py:27
  200.7 3.9 %copy-start.5 = (bf16[256,2048]{1,0:T(8,128)(2,1)}, bf16[256,2048]{1,0:T(8,128)(2,1)S(1)}, u32[]{:S(2)}) copy-start(bf16[256,2048]{1,0:T(8,128)(2,1)S(1)} %collective-permute-done.1) | copy-start | bytes 3145732
  204.7 3.8 %collective-permute-start.2 = (bf16[256,2048]{1,0:T(8,128)(2,1)}, bf16[256,2048]{1,0:T(8,128)(2,1)}, u32[]{:S(2)}, u32[]{:S(2)}) collective-permute-start(bf16[256,2048]{1,0:T(8,128)(2,1)} %multiply_convert_fusion.3), channel_id=1, source_target_pairs={{0,1},{1,0},{2,3},{3,2},{4,5},{5,4},{6,7},{7,6},{8,9},{9,8},{10,11... | collective-permute-start | bytes 3145736 | tf_op jit(solution)/shard_map/ppermute | solution.py:27
  206.6 1.8 copy-start.19
  206.6 1.8 copy-start.15
  206.6 1.9 copy-start.11
  208.5 2.4 copy-start.10
  218.5 1.3 copy-start.17
  218.5 3.6 %copy-start.4 = (bf16[1,256,2048]{2,1,0:T(8,128)(2,1)S(1)}, bf16[1,256,2048]{2,1,0:T(8,128)(2,1)}, u32[]{:S(2)}) copy-start(bf16[1,256,2048]{2,1,0:T(8,128)(2,1)} %param.12) | copy-start | bytes 3145732
  218.5 3.6 %copy-start.6 = (bf16[256,2048]{1,0:T(8,128)(2,1)S(1)}, bf16[256,2048]{1,0:T(8,128)(2,1)}, u32[]{:S(2)}) copy-start(bf16[256,2048]{1,0:T(8,128)(2,1)} %copy-done.5) | copy-start | bytes 3145732
  218.5 3.6 %copy-start.8 = (bf16[512,2048]{1,0:T(8,128)(2,1)S(1)}, bf16[512,2048]{1,0:T(8,128)(2,1)}, u32[]{:S(2)}) copy-start(bf16[512,2048]{1,0:T(8,128)(2,1)} %convolution_convert_fusion.2) | copy-start | bytes 6291460
  219.3 2.7 %collective-permute-start.3 = (bf16[256,2048]{1,0:T(8,128)(2,1)S(1)}, bf16[256,2048]{1,0:T(8,128)(2,1)S(1)}, u32[]{:S(2)}, u32[]{:S(2)}) collective-permute-start(bf16[256,2048]{1,0:T(8,128)(2,1)S(1)} %slice.338), channel_id=1, source_target_pairs={{0,1},{1,0},{2,3},{3,2},{4,5},{5,4},{6,7},{7,6},{8,9},{9,8},{10,11... | collective-permute-start | bytes 3145736 | tf_op jit(solution)/shard_map/ppermute | solution.py:27
  219.8 7.3 %slice-start = ((s8[5767168]{0:T(1024)(128)(4,1)}), s8[4194304]{0:T(1024)(128)(4,1)S(1)}, s32[]{:S(2)}) async-start(s8[5767168]{0:T(1024)(128)(4,1)} %bitcast.115), calls=%async_computation | async-start | bytes 8388608
  219.8 7.3 %slice-start.1 = ((s8[5767168]{0:T(1024)(128)(4,1)}), s8[1572864]{0:T(1024)(128)(4,1)S(1)}, s32[]{:S(2)}) async-start(s8[5767168]{0:T(1024)(128)(4,1)} %bitcast.115), calls=%async_computation.1 | async-start | bytes 3145728
  223.3 2.7 %collective-permute-start.4 = (bf16[256,2048]{1,0:T(8,128)(2,1)S(1)}, bf16[256,2048]{1,0:T(8,128)(2,1)S(1)}, u32[]{:S(2)}, u32[]{:S(2)}) collective-permute-start(bf16[256,2048]{1,0:T(8,128)(2,1)S(1)} %multiply_convert_fusion.2), channel_id=1, source_target_pairs={{0,1},{1,0},{2,3},{3,2},{4,5},{5,4},{6,7},{7,6},{8,9},{9,8},{10,11... | collective-permute-start | bytes 3145736 | tf_op jit(solution)/shard_map/ppermute | solution.py:27
  226.1 1.0 copy-start.18
  245.8 4.2 %copy-start.9 = (bf16[512,2048]{1,0:T(8,128)(2,1)S(1)}, bf16[512,2048]{1,0:T(8,128)(2,1)}, u32[]{:S(2)}) copy-start(bf16[512,2048]{1,0:T(8,128)(2,1)} %convolution_convert_fusion.1) | copy-start | bytes 6291460
  247.2 2.7 %collective-permute-start.5 = (bf16[256,2048]{1,0:T(8,128)(2,1)S(1)}, bf16[256,2048]{1,0:T(8,128)(2,1)S(1)}, u32[]{:S(2)}, u32[]{:S(2)}) collective-permute-start(bf16[256,2048]{1,0:T(8,128)(2,1)S(1)} %slice.340), channel_id=1, source_target_pairs={{0,1},{1,0},{2,3},{3,2},{4,5},{5,4},{6,7},{7,6},{8,9},{9,8},{10,11... | collective-permute-start | bytes 3145736 | tf_op jit(solution)/shard_map/ppermute | solution.py:27

commit v2 on v1

--- a/solution.py
+++ b/solution.py
@@ -11,6 +11,12 @@
 CHAN_EPS = 0.02
 MESH = pl.DeviceIdType.MESH
 CHUNKS = 8
+LANES = 128
+ROW_BLOCK = 32
+CONV_BLOCK = 64
+PAD = 32
+FIRST_SLOT = 6
+SECOND_SLOT = 4
 SHARES = ((6, 5), (6, 4), (6, 5), (6, 5))
 UP, DOWN, OVER_X, OVER_Y = range(4)
 
@@ -67,17 +73,17 @@
             return {"rep": 1 - self.x}
         return {"fs": self.z * 2 + 1 - self.y}
 
-    def barrier(self):
+    def barrier(self, *others):
         barrier = pltpu.get_barrier_semaphore()
-        for way in (OVER_X, OVER_Y):
-            pl.semaphore_signal(barrier, inc=1, device_id=self.target(way), device_id_type=MESH)
+        for target in (self.target(OVER_X), self.target(OVER_Y), *others):
+            pl.semaphore_signal(barrier, inc=1, device_id=target, device_id_type=MESH)
         for way, present in ((UP, self.has_up), (DOWN, self.has_down)):
 
             @pl.when(present)
             def _(way=way):
                 pl.semaphore_signal(barrier, inc=1, device_id=self.target(way), device_id_type=MESH)
 
-        peers = 2 + self.has_up.astype(jnp.int32) + self.has_down.astype(jnp.int32)
+        peers = 2 + len(others) + self.has_up.astype(jnp.int32) + self.has_down.astype(jnp.int32)
         pl.semaphore_wait(barrier, peers)
 
     def count(self, m):
@@ -93,8 +99,14 @@
         flip = self.x if mine else 1 - self.x
         return pl.ds(first + flip * (count - last - first), last - first)
 
-    def local(self, m):
-        return pltpu.make_async_copy(self.ins[m], self.slots[m].at[self.own], self.local_sems.at[m])
+    def locals(self, m):
+        copies, first = [], 0
+        for n, part in enumerate(self.ins[m]):
+            height = part.shape[1]
+            here = self.slots[m].at[self.own, :, pl.ds(first, height)]
+            copies.append(pltpu.make_async_copy(part, here, self.local_sems.at[m, n]))
+            first += height
+        return copies
 
     def copy(self, m, k, c, way):
         piece = self.slots[m].at[k, c]
@@ -111,20 +123,23 @@
     def spread(self, m, k, e, ways):
         c = self.chunk(m, e)
         for way, wanted in ways:
-            if wanted is True:
-                self.copy(m, k, c, way).start()
-            elif wanted is not False:
-                pl.when(wanted)(lambda way=way: self.copy(m, k, c, way).start())
+            pl.when(wanted)(lambda way=way: self.copy(m, k, c, way).start())
 
     def start_local(self):
         for m in range(len(self.ins)):
-            self.local(m).start()
+            for part in self.locals(m):
+                part.start()
 
     def start_own(self, m):
         along, across = self.shares[m]
-        self.local(m).wait()
-        for e in range(along):
+        for part in self.locals(m):
+            part.wait()
+
+        def step(e, carry):
             self.spread(m, self.own, e, ((UP, self.has_up), (DOWN, self.has_down), (OVER_Y, e < across)))
+            return carry
+
+        lax.fori_loop(0, along, step, 0)
 
     def pieces(self, d):
         return ((self.z - d, self.z - d >= 0, self.has_up, UP), (self.z + d, self.z + d < self.depth, self.has_down, DOWN))
@@ -152,27 +167,24 @@
                 self.copy(m, k, self.chunk(m, e), OVER_Y).wait_recv()
                 self.spread(m, k, e, ((OVER_X, e < spare),))
 
-    def run(self):
-        total = len(self.ins)
-        self.start_own(0)
-        for m in range(total):
-            along, across = self.shares[m]
-
-            def step(r, carry, m=m, along=along, across=across):
-                if m + 1 < total:
-
-                    @pl.when(r == max(self.depth - 2, 0))
-                    def _():
-                        self.start_own(m + 1)
-
-                for e in range(max(along, across)):
-                    if e < along:
-                        self.arrive_along(m, r + 1, e)
-                    if e < across:
-                        self.arrive_across(m, r, e)
-                return carry
-
-            lax.fori_loop(0, self.depth, step, 0)
+    def slots_of(self, m):
+        return self.depth * self.shares[m][0]
+
+    def run(self, m, work=None):
+        along, across = self.shares[m]
+        ahead = max(self.depth - 2, 0) * along
+
+        def step(t, carry):
+            r, e = lax.div(t, along), lax.rem(t, along)
+            if m + 1 < len(self.ins):
+                pl.when(t == ahead)(lambda: self.start_own(m + 1))
+            self.arrive_along(m, r + 1, e)
+            pl.when(e < across)(lambda: self.arrive_across(m, r, e))
+            if work is not None:
+                work(t)
+            return carry
+
+        lax.fori_loop(0, self.slots_of(m), step, 0)
 
     def side(self, m, k, first, last, mine):
         piece = self.slots[m].at[k, self.chunks(m, first, last, mine)]
@@ -196,64 +208,76 @@
             device_id_type=MESH,
         )
 
-    def drain(self):
-        for m in range(len(self.ins)):
-            along, across = self.shares[m]
-            count = self.count(m)
-
-            def step(d, carry, m=m, along=along, across=across, count=count):
-                for side, (at, present, further, way) in enumerate(self.pieces(d)):
-                    if side == 1:
-                        present = jnp.logical_and(present, d > 0)
-
-                    @pl.when(present)
-                    def _(at=at, further=further, way=way):
-                        k, cross = at * 2 + self.y, at * 2 + 1 - self.y
-
-                        @pl.when(d > 0)
-                        def _():
-                            self.side(m, k, 0, count - along, False).wait_recv()
-                            self.side(m, k, 0, count - along, True).wait_send()
-
-                        self.side(m, cross, 0, count - across, False).wait_recv()
-                        self.side(m, cross, 0, count - across, True).wait_send()
-                        self.sent(m, k, across, OVER_Y).wait_send()
-                        pl.when(further)(lambda: self.sent(m, k, along, way).wait_send())
-
-                return carry
-
-            lax.fori_loop(0, self.depth, step, 0)
-
-            @pl.when(self.has_down)
-            def _(m=m, along=along):
-                self.sent(m, self.own, along, DOWN).wait_send()
+    def every(self, visit):
+        def step(d, carry):
+            for side, (at, present, further, way) in enumerate(self.pieces(d)):
+                if side == 1:
+                    present = jnp.logical_and(present, d > 0)
+                pl.when(present)(lambda at=at, further=further, way=way: visit(d, at, further, way))
+            return carry
+
+        lax.fori_loop(0, self.depth, step, 0)
+
+    def settle(self, m):
+        along, across = self.shares[m]
+        count = self.count(m)
+
+        def visit(d, at, further, way):
+            k, cross = at * 2 + self.y, at * 2 + 1 - self.y
+            pl.when(d > 0)(lambda: self.side(m, k, 0, count - along, False).wait_recv())
+            self.side(m, cross, 0, count - across, False).wait_recv()
+
+        self.every(visit)
+
+    def drain(self, m):
+        along, across = self.shares[m]
+        count = self.count(m)
+
+        def visit(d, at, further, way):
+            k, cross = at * 2 + self.y, at * 2 + 1 - self.y
+            pl.when(d > 0)(lambda: self.side(m, k, 0, count - along, True).wait_send())
+            self.side(m, cross, 0, count - across, True).wait_send()
+            self.sent(m, k, across, OVER_Y).wait_send()
+            pl.when(further)(lambda: self.sent(m, k, along, way).wait_send())
+
+        self.every(visit)
+        pl.when(self.has_down)(lambda: self.sent(m, self.own, along, DOWN).wait_send())
+
+
+def gather_sems(total, parts, counts):
+    dma = pltpu.SemaphoreType.DMA
+    return (
+        [dma((len(counts), parts))]
+        + [dma((total, count)) for count in counts]
+        + [dma((total,)) for _ in counts]
+        + [dma((4, total)) for _ in counts]
+    )
 
 
 def gather_kernel(depth, shares, count, *refs):
-    ins, slots = refs[:count], refs[count : 2 * count]
+    ins, slots = [(ref,) for ref in refs[:count]], refs[count : 2 * count]
     sems = refs[2 * count :]
-    local_sems, sems = sems[0], sems[1:]
-    gather = Gather(depth, shares, ins, slots, local_sems, sems[:count], sems[count : 2 * count], sems[2 * count :])
+    gather = Gather(depth, shares, ins, slots, sems[0], *(sems[1 + i * count : 1 + (i + 1) * count] for i in range(3)))
     gather.start_local()
     gather.barrier()
-    gather.run()
-    gather.drain()
+    gather.start_own(0)
+    for m in range(count):
+        gather.run(m)
+    for m in range(count):
+        gather.settle(m)
+        gather.drain(m)
 
 
 def gather_all(blocks, shares):
     total = lax.axis_size("fs")
     count = len(blocks)
     outs = [jax.ShapeDtypeStruct((total, *b.shape), b.dtype) for b in blocks]
-    dma = pltpu.SemaphoreType.DMA
     return pl.pallas_call(
         functools.partial(gather_kernel, total // 2, shares, count),
         out_shape=outs,
         in_specs=[pl.BlockSpec(memory_space=pl.ANY)] * count,
         out_specs=[pl.BlockSpec(memory_space=pltpu.VMEM)] * count,
-        scratch_shapes=[dma((count,))]
-        + [dma((total, b.shape[0])) for b in blocks]
-        + [dma((total,)) for b in blocks]
-        + [dma((4, total)) for b in blocks],
+        scratch_shapes=gather_sems(total, 1, [b.shape[0] for b in blocks]),
         compiler_params=pltpu.CompilerParams(
             collective_id=0, has_side_effects=True, vmem_limit_bytes=48 * 2**20
         ),
@@ -283,6 +307,362 @@
 
 def chunked(block, pieces):
     return block.reshape(pieces, block.shape[0] // pieces, block.shape[1])
+
+
+class Layer:
+    def __init__(self, gather, tokens, gains, taps, gain, out, scratch):
+        self.gather = gather
+        self.tokens, self.gains, self.taps, self.gain, self.out = tokens, gains, taps, gain, out
+        (
+            self.own,
+            self.stream,
+            self.rows,
+            self.hidden,
+            self.partial,
+            self.landed,
+            self.padded,
+            self.conv,
+            self.sums,
+            self.act,
+            self.own_sem,
+            self.row_send,
+            self.row_recv,
+            self.part_send,
+            self.part_recv,
+            self.sum_send,
+            self.sum_recv,
+        ) = scratch
+        self.half, self.width = self.own.shape
+        self.units = self.hidden.shape[1]
+        self.total = gather.depth * 2
+        self.piece = self.width // self.total
+        self.tp = lax.axis_index("tp")
+        self.partner = {"tp": 1 - self.tp}
+        self.mine = pl.multiple_of(self.tp * self.half, self.half)
+        self.theirs = pl.multiple_of((1 - self.tp) * self.half, self.half)
+
+    def remote(self, src, dst, send_sem, recv_sem):
+        return pltpu.make_async_remote_copy(
+            src_ref=src,
+            dst_ref=dst,
+            send_sem=send_sem,
+            recv_sem=recv_sem,
+            device_id=self.partner,
+            device_id_type=MESH,
+        )
+
+    def row_copy(self, n, start=None):
+        here = self.rows.at[n, pl.ds(self.mine if start is None else start, self.half)]
+        return self.remote(here, here, self.row_send.at[n], self.row_recv.at[n])
+
+    def part_copy(self, n, k):
+        cols = pl.ds(pl.multiple_of(k * self.piece, self.piece), self.piece)
+        return self.remote(
+            self.partial.at[n, pl.ds(self.theirs, self.half), cols],
+            self.landed.at[n, :, cols],
+            self.part_send.at[n, k],
+            self.part_recv.at[n, k],
+        )
+
+    def sum_copy(self):
+        return self.remote(self.sums.at[0], self.sums.at[1], self.sum_send.at[0], self.sum_recv.at[0])
+
+    def norm(self, n, first, stream):
+        square_mean = jnp.mean(stream * stream, axis=-1, keepdims=True)
+        scaled = stream * lax.rsqrt(square_mean + ROW_EPS) * self.gains[n][...].astype(jnp.float32)
+        self.rows[n, pl.ds(self.mine + first, stream.shape[0]), :] = scaled.astype(jnp.bfloat16)
+
+    def block(self, i):
+        return pl.multiple_of(i * ROW_BLOCK, ROW_BLOCK)
+
+    def start_rows(self):
+        def step(i, carry):
+            first = self.block(i)
+            self.norm(0, first, self.own[pl.ds(first, ROW_BLOCK), :].astype(jnp.float32))
+            return carry
+
+        lax.fori_loop(0, self.half // ROW_BLOCK, step, 0)
+        self.row_copy(0).start()
+
+    def update(self, n, i, scale):
+        first = self.block(i)
+        here = pl.ds(first, ROW_BLOCK)
+        before = self.own[here, :].astype(jnp.float32) if n == 0 else self.stream[here, :]
+        added = self.partial[n, pl.ds(self.mine + first, ROW_BLOCK), :].astype(jnp.float32) + self.landed[
+            n, here, :
+        ].astype(jnp.float32)
+        stream = before + (added if scale is None else scale * added)
+        self.stream[here, :] = stream
+        self.norm(n + 1, first, stream)
+
+    def await_parts(self, n):
+        def step(k, carry):
+            self.part_copy(n, k).wait_recv()
+            return carry
+
+        lax.fori_loop(0, self.total, step, 0)
+
+    def matrix(self, m, first, size):
+        return self.gather.slots[m][:, :, :, pl.ds(first, size)].reshape(self.width, size)
+
+    def hidden_tile(self, n, row, height, first, size):
+        rows = self.rows[n, pl.ds(row, height), :]
+        gate = jnp.dot(rows, self.matrix(0, first, size), preferred_element_type=jnp.float32)
+        up = jnp.dot(rows, self.matrix(1, first, size), preferred_element_type=jnp.float32)
+        self.hidden[pl.ds(row, height), pl.ds(first, size)] = (jax.nn.silu(gate) * up).astype(jnp.bfloat16)
+
+    def down_piece(self, n, k):
+        weights = self.gather.slots[2][k].reshape(self.units, self.piece)
+        result = jnp.dot(self.hidden[...], weights, preferred_element_type=jnp.float32)
+        cols = pl.ds(pl.multiple_of(k * self.piece, self.piece), self.piece)
+        self.partial[n, :, cols] = result.astype(jnp.bfloat16)
+        self.part_copy(n, k).start()
+
+    def first_work(self, t):
+        j = t - FIRST_SLOT
+
+        @pl.when(j == 0)
+        def _():
+            self.gather.settle(0)
+            self.gather.settle(1)
+            self.row_copy(0, self.theirs).wait_recv()
+
+        @pl.when(jnp.logical_and(j >= 0, j < self.units // LANES))
+        def _():
+            self.hidden_tile(0, 0, 2 * self.half, pl.multiple_of(j * LANES, LANES), LANES)
+
+    def second_work(self, t):
+        j = t - SECOND_SLOT
+        blocks = self.half // ROW_BLOCK
+        i = j - self.total
+        pl.when(j == 0)(lambda: self.gather.settle(2))
+        pl.when(jnp.logical_and(j >= 0, i < 0))(lambda: self.down_piece(0, j))
+        pl.when(i == 0)(lambda: self.await_parts(0))
+        pl.when(jnp.logical_and(i >= 0, i < blocks))(lambda: self.update(0, i, 0.5))
+        pl.when(i == blocks - 1)(lambda: self.row_copy(1).start())
+
+    def small(self, n):
+        height = self.gather.slots[3].shape[2] // 3
+        return (pl.ds(n * height, height),)
+
+    def gated(self, row):
+        rows = self.rows[1, pl.ds(row, self.half), :]
+        value_at, gate_at = self.small(0)[0], self.small(1)[0]
+        whole = self.gather.slots[3]
+        value = whole[:, :, value_at, :].reshape(self.width, -1)
+        gate = whole[:, :, gate_at, :].reshape(self.width, -1)
+        values = jnp.dot(rows, value, preferred_element_type=jnp.float32)
+        gates = jnp.dot(rows, gate, preferred_element_type=jnp.float32)
+        self.padded[pl.ds(PAD + row, self.half), :] = values * jax.nn.sigmoid(gates)
+
+    def convolve(self):
+        taps = self.taps.shape[0]
+        lanes = self.sums.shape[-1]
+
+        def step(i, carry):
+            first = pl.multiple_of(i * CONV_BLOCK, CONV_BLOCK)
+            window = self.padded[pl.ds(first, CONV_BLOCK + PAD), :]
+            total = jnp.zeros((CONV_BLOCK, window.shape[1]), jnp.float32)
+            for j in range(taps):
+                at = PAD - (taps - 1) + j
+                total = total + window[at : at + CONV_BLOCK] * self.taps[j : j + 1, :].astype(jnp.float32)
+            here = pl.ds(first, CONV_BLOCK)
+            self.conv[here, :] = total
+            plain = jnp.sum(total, axis=-1, keepdims=True)
+            squared = jnp.sum(total * total, axis=-1, keepdims=True)
+            lane = lax.broadcasted_iota(jnp.int32, (CONV_BLOCK, lanes), 1)
+            self.sums[0, here, :] = jnp.where(lane < lanes // 2, plain, squared)
+            return carry
+
+        lax.fori_loop(0, 2 * self.half // CONV_BLOCK, step, 0)
+
+    def activate(self):
+        lanes = self.sums.shape[-1]
+        channels = 2 * self.conv.shape[1]
+
+        def step(i, carry):
+            here = pl.ds(pl.multiple_of(i * CONV_BLOCK, CONV_BLOCK), CONV_BLOCK)
+            sums = (self.sums[0, here, :] + self.sums[1, here, :]) / channels
+            average, square = sums[:, :1], sums[:, lanes // 2 : lanes // 2 + 1]
+            spread = jnp.maximum(square - average * average, 0.0)
+            scaled = (self.conv[here, :] - average) * lax.rsqrt(spread + CHAN_EPS) * self.gain[...].astype(jnp.float32)
+            self.act[here, :] = jax.nn.silu(scaled).astype(jnp.bfloat16)
+            return carry
+
+        lax.fori_loop(0, 2 * self.half // CONV_BLOCK, step, 0)
+
+    def mix(self):
+        at = self.small(2)[0]
+
+        def step(k, carry):
+            weights = self.gather.slots[3][k, :, at, :].reshape(-1, self.piece)
+            result = jnp.dot(self.act[...], weights, preferred_element_type=jnp.float32)
+            cols = pl.ds(pl.multiple_of(k * self.piece, self.piece), self.piece)
+            self.partial[1, :, cols] = result.astype(jnp.bfloat16)
+            self.part_copy(1, k).start()
+            return carry
+
+        lax.fori_loop(0, self.total, step, 0)
+
+    def conv_module(self):
+        self.padded[:PAD, :] = jnp.zeros((PAD, self.padded.shape[1]), jnp.float32)
+        self.gated(self.mine)
+        self.row_copy(1, self.theirs).wait_recv()
+        self.gated(self.theirs)
+        self.convolve()
+        self.sum_copy().start()
+        self.sum_copy().wait_recv()
+        self.activate()
+        self.mix()
+        self.await_parts(1)
+
+        def step(i, carry):
+            self.update(1, i, None)
+            return carry
+
+        lax.fori_loop(0, self.half // ROW_BLOCK, step, 0)
+        self.row_copy(2).start()
+
+    def second_half_step(self):
+        tile = 2 * LANES
+        whole = self.units // tile
+        early = min(2, whole)
+
+        def split(i, carry):
+            pl.when(i == early)(lambda: self.row_copy(2, self.theirs).wait_recv())
+            row = jnp.where(i < early, self.mine, self.theirs)
+            first = pl.multiple_of(lax.rem(i, early) * tile, tile)
+            self.hidden_tile(2, pl.multiple_of(row, self.half), self.half, first, tile)
+            return carry
+
+        lax.fori_loop(0, 2 * early, split, 0)
+
+        def step(j, carry):
+            self.hidden_tile(2, 0, 2 * self.half, pl.multiple_of(j * tile, tile), tile)
+            return carry
+
+        lax.fori_loop(early, whole, step, 0)
+        if self.units % tile:
+            self.hidden_tile(2, 0, 2 * self.half, whole * tile, self.units % tile)
+
+        def piece(k, carry):
+            self.down_piece(2, k)
+            return carry
+
+        lax.fori_loop(0, self.total, piece, 0)
+
+        def finish(k, carry):
+            self.part_copy(2, k).wait_recv()
+            cols = pl.ds(pl.multiple_of(k * self.piece, self.piece), self.piece)
+            added = self.partial[2, pl.ds(self.mine, self.half), cols].astype(jnp.float32) + self.landed[
+                2, :, cols
+            ].astype(jnp.float32)
+            self.out[:, cols] = (self.stream[:, cols] + 0.5 * added).astype(self.out.dtype)
+            return carry
+
+        lax.fori_loop(0, self.total, finish, 0)
+
+    def run(self):
+        gather = self.gather
+        own = pltpu.make_async_copy(self.tokens, self.own, self.own_sem.at[0])
+        gather.start_local()
+        own.start()
+        gather.barrier(self.partner)
+        gather.start_own(0)
+        own.wait()
+        self.start_rows()
+        gather.run(0)
+        gather.run(1)
+        gather.run(2, self.first_work)
+        gather.run(3, self.second_work)
+        gather.settle(3)
+        self.conv_module()
+        self.second_half_step()
+        for m in range(len(gather.ins)):
+            gather.drain(m)
+        self.sum_copy().wait_send()
+
+        def step(n, carry):
+            self.row_copy(n).wait_send()
+
+            def piece(k, inner):
+                self.part_copy(n, k).wait_send()
+                return inner
+
+            return lax.fori_loop(0, self.total, piece, carry)
+
+        lax.fori_loop(0, 3, step, 0)
+
+
+def layer_kernel(depth, *refs):
+    tokens, gains, refs = refs[0], refs[1:4], refs[4:]
+    ins, refs = ((refs[0],), (refs[1],), (refs[2],), refs[3:6]), refs[6:]
+    taps, gain, out, refs = refs[0], refs[1], refs[2], refs[3:]
+    slots, sems, scratch = refs[:4], refs[4:17], refs[17:]
+    gather = Gather(depth, SHARES, ins, slots, sems[0], sems[1:5], sems[5:9], sems[9:13])
+    Layer(gather, tokens, gains, taps, gain, out, scratch).run()
+
+
+def fused_layer(tokens, gains, blocks, smalls, depthwise, conv_gain):
+    total = lax.axis_size("fs")
+    half, width = tokens.shape
+    units, channels = blocks[0].shape[2], depthwise.shape[1]
+    vmem, dma = pltpu.VMEM, pltpu.SemaphoreType.DMA
+    merged = (smalls[0].shape[0], 3 * smalls[0].shape[1], smalls[0].shape[2])
+    shapes = [b.shape for b in blocks] + [merged]
+    f32, bf16 = jnp.float32, jnp.bfloat16
+    any_space, in_vmem = pl.BlockSpec(memory_space=pl.ANY), pl.BlockSpec(memory_space=pltpu.VMEM)
+    return pl.pallas_call(
+        functools.partial(layer_kernel, total // 2),
+        out_shape=jax.ShapeDtypeStruct((half, width), bf16),
+        in_specs=[any_space] + [in_vmem] * 3 + [any_space] * 6 + [in_vmem] * 2,
+        out_specs=in_vmem,
+        scratch_shapes=[vmem((total, *shape), bf16) for shape in shapes]
+        + gather_sems(total, 3, [shape[0] for shape in shapes])
+        + [
+            vmem((half, width), bf16),
+            vmem((half, width), f32),
+            vmem((3, 2 * half, width), bf16),
+            vmem((2 * half, units), bf16),
+            vmem((3, 2 * half, width), bf16),
+            vmem((3, half, width), bf16),
+            vmem((PAD + 2 * half, channels), f32),
+            vmem((2 * half, channels), f32),
+            vmem((2, 2 * half, LANES), f32),
+            vmem((2 * half, channels), bf16),
+            dma((1,)),
+            dma((3,)),
+            dma((3,)),
+            dma((3, total)),
+            dma((3, total)),
+            dma((1,)),
+            dma((1,)),
+        ],
+        compiler_params=pltpu.CompilerParams(
+            collective_id=0, has_side_effects=True, vmem_limit_bytes=60 * 2**20
+        ),
+        name="fused_layer",
+    )(tokens, *gains, *blocks, *smalls, depthwise, conv_gain)
+
+
+def fits(half, ffn_gate, ffn_down, conv_value, conv_out, depthwise):
+    piece, total = ffn_gate.shape[0], lax.axis_size("fs")
+    slots = total // 2 * SHARES[0][0]
+    return (
+        piece % (16 * CHUNKS) == 0
+        and ffn_down.shape[0] % (16 * CHUNKS) == 0
+        and conv_out.shape[0] == piece
+        and conv_value.shape[1] == piece
+        and piece % LANES == 0
+        and ffn_gate.shape[1] % LANES == 0
+        and half % ROW_BLOCK == 0
+        and half % CONV_BLOCK == 0
+        and depthwise.shape[0] <= PAD
+        and slots >= FIRST_SLOT + ffn_gate.shape[1] // LANES
+        and slots >= SECOND_SLOT + total + half // ROW_BLOCK
+        and lax.axis_size("tp") == 2
+        and lax.axis_size("rep") == 2
+    )
 
 
 def shards(
@@ -300,6 +680,16 @@
     conv_out,
 ):
     width = tokens.shape[-1]
+    if fits(tokens.size // width, ffn_gate, ffn_down, conv_value, conv_out, depthwise):
+        mixed = fused_layer(
+            tokens.reshape(-1, width),
+            [gain.reshape(1, -1) for gain in (norm_first, norm_mixer, norm_second)],
+            [chunked(block, CHUNKS) for block in (ffn_gate, ffn_up, ffn_down)],
+            [chunked(block, CHUNKS) for block in (conv_value, conv_gate, conv_out)],
+            depthwise,
+            conv_gain.reshape(1, -1),
+        )
+        return mixed.reshape(tokens.shape)
     stream = tokens.reshape(-1, width).astype(jnp.float32)
     first_rows = widen(rms_rows(stream, norm_first))
     small = jnp.concatenate([conv_value, conv_gate, conv_out.reshape(-1, conv_value.shape[1])])

time: 252 us -> 188 us (0.75)
  matrix products: 46.3 us -> 0 us
  Pallas kernels: 161 us -> 182 us
  other arithmetic: 14.3 us -> 0 us
  local copies, waits for them, and re-layouts: 15.9 us -> 5.53 us
  waiting for transfers between devices: 9.56 us -> 0 us
    dot_general x7 -> x0, matrix products: 46.3 us -> none  [the longest x1 14 us: shards(): jnp.dot(hidden, whole_down, preferred_element_type=jnp.float32)]
    pallas_call x1, Pallas kernels: 161 us -> 182 us  [fused_layer(): pl.pallas_call(functools.partial(layer_kernel, total // 2), out_shape=jax...]
    ppermute x6 -> x0, waiting for transfers between devices: 9.56 us -> none  [swap(): return lax.ppermute(value, 'tp', [(i, size - 1 - i) for i in range(size)])]
    reduce_sum x4 -> x0, other arithmetic: 7.12 us -> none  [the longest x3 4.75 us: rms_rows(): square_mean = jnp.mean(stream * stream, axis=-1, keepdims=True)]
    reshape x1 -> x4, local copies, waits for them, and re-layouts: 8.26 us -> 2.39 us  [the longest x3 1.82 us: shards(): gain.reshape(1, -1)]
    convert_element_type x8 -> x0, other arithmetic: 5.54 us -> none  [the longest x3 4.44 us: rms_rows(): (stream * lax.rsqrt(square_mean + ROW_EPS) * gain_vec.astype(jnp.float32)...]
    slice x8 -> x0, local copies, waits for them, and re-layouts: 4.81 us -> none  [the longest x3 2.89 us: narrow(): rounded[half:]]
  transfers between devices with their start and end apart: 6 -> 0, of which waited for: 4 -> 0; matrix products, arithmetic and copies ran while one was open for 5% -> 0% of each run, Pallas kernels for 64% -> 0%
where the time goes in v2:
time: 188 us
  Pallas kernels  182 us (97%)
  local copies, waits for them, and re-layouts  5.53 us (3%)
    pallas_call x1, Pallas kernels, fused_layer(): pl.pallas_call(functools.partial(layer_kernel, total // 2), out_shape=jax...  182 us

profile of v2, /device:TPU:0, one launch (start us, length us, event | category | flops | bytes accessed | tf_op | source)
XLA Modules:
  0.0 187.7 jit_solution(9319195757912258159)
XLA Ops:
  0.0 0.0 copy-start
  0.0 0.0 copy-start.3
  0.0 0.7 copy-done.3
  0.7 0.6 reshape.46.refs_11_
  1.2 0.0 copy-done
  1.2 0.0 copy-start.1
  1.3 0.6 reshape.37.refs_1_
  1.9 0.1 copy-done.1
  1.9 0.0 copy-start.2
  1.9 0.6 reshape.38.refs_2_
  2.6 0.1 copy-done.2
  2.6 0.6 reshape.39.refs_3_
  3.2 182.1 %fused_layer.1 = bf16[256,2048]{1,0:T(8,128)(2,1)} custom-call(bf16[256,2048]{1,0:T(8,128)(2,1)} %bitcast.9, bf16[1,2048]{1,0:T(2,128)(2,1)} %reshape.37.refs_1_, bf16[1,2048]{1,0:T(2,128)(2,1)} %reshape.38.refs_2_, bf16[1,2048]{1,0:T(2,128)(2,1)} %reshape.39.refs_3_, bf16[8,32,1408]{2,1,0:T(8,128)(2,1)} %bitcast.10, bf16[8,32,1408]{2,1,0:T(8,128)(2,1)} %bitcast.11, ...), custom_call_target="tpu_custom_call" | custom-call | tf_op jit(solution)/shard_map/fused_layer/pallas_call | solution.py:615
  185.4 2.3 %copy.14 = bf16[1,256,2048]{2,1,0:T(8,128)(2,1)} copy(bf16[1,256,2048]{2,1,0:T(8,128)(2,1)} %bitcast.8) | data formatting | bytes 2097152
Async XLA Ops:
  0.0 1.2 copy-start
  0.0 0.7 copy-start.3
  1.2 0.7 copy-start.1
  1.9 0.7 copy-start.2

commit v3 on v2

v3 whole, which is shorter than its diff:
```python
import functools

import jax
import jax.numpy as jnp
from jax import lax
from jax.experimental import pallas as pl
from jax.experimental.pallas import tpu as pltpu
from jax.sharding import PartitionSpec as P

ROW_EPS = 0.05
CHAN_EPS = 0.02
MESH = pl.DeviceIdType.MESH
CHUNKS = 8
CONV_CHUNKS = 4
LANES = 128
ROW_BLOCK = 32
CONV_BLOCK = 64
PAD = 32
SUBLANES = 8
FIRST_SLOT = 8
SECOND_SLOT = 2
THIRD_SLOT = 2
PER_SLOT = 2
UP, DOWN, OVER_X, OVER_Y = range(4)


def rms_rows(stream, gain_vec):
    square_mean = jnp.mean(stream * stream, axis=-1, keepdims=True)
    return (stream * lax.rsqrt(square_mean + ROW_EPS) * gain_vec.astype(jnp.float32)).astype(
        jnp.bfloat16
    )


def swap(value):
    size = lax.axis_size("tp")
    return lax.ppermute(value, "tp", [(i, size - 1 - i) for i in range(size)])


def widen(normed):
    return jnp.concatenate([normed, swap(normed)])


def narrow(partial_value):
    rounded = partial_value.astype(jnp.bfloat16)
    half = rounded.shape[0] // 2
    return rounded[:half].astype(jnp.float32) + swap(rounded[half:]).astype(jnp.float32)


def reorder(rows):
    half = rows.shape[0] // 2
    flipped = jnp.concatenate([rows[half:], rows[:half]])
    return jnp.where(lax.axis_index("tp") == 0, rows, flipped)


def place():
    fs = lax.axis_index("fs")
    return lax.axis_index("rep"), lax.rem(fs, 2), fs // 2


class Gather:
    def __init__(self, depth, ins, slots, local_sems, side_sems, send_sems, recv_sems):
        self.depth = depth
        self.ins, self.slots = ins, slots
        self.local_sems, self.recv_sems = local_sems, recv_sems
        self.side_sems, self.send_sems = side_sems, send_sems
        self.x, self.y, self.z = place()
        self.has_up, self.has_down = self.z + 1 < depth, self.z > 0
        self.own = self.z * 2 + self.y

    def target(self, way):
        if way == UP:
            return {"fs": (self.z + 1) * 2 + self.y}
        if way == DOWN:
            return {"fs": (self.z - 1) * 2 + self.y}
        if way == OVER_X:
            return {"rep": 1 - self.x}
        return {"fs": self.z * 2 + 1 - self.y}

    def barrier(self, *others):
        barrier = pltpu.get_barrier_semaphore()
        for target in (self.target(OVER_X), self.target(OVER_Y), *others):
            pl.semaphore_signal(barrier, inc=1, device_id=target, device_id_type=MESH)
        for way, present in ((UP, self.has_up), (DOWN, self.has_down)):

            @pl.when(present)
            def _(way=way):
                pl.semaphore_signal(barrier, inc=1, device_id=self.target(way), device_id_type=MESH)

        peers = 2 + len(others) + self.has_up.astype(jnp.int32) + self.has_down.astype(jnp.int32)
        pl.semaphore_wait(barrier, peers)

    def count(self, m):
        return self.slots[m].shape[0] // (2 * self.depth)

    def at_end(self, at):
        return jnp.logical_or(at == 0, at == self.depth - 1)

    def along(self, m, at):
        count = self.count(m)
        return jnp.where(self.at_end(at), count - count // 4, count)

    def across(self, m, d):
        count = self.count(m)
        far = jnp.clip(count // 2 + d - 1, count // 2, count - count // 4)
        return jnp.where(self.at_end(self.z), far, count // 2)

    def chunk(self, m, k, e):
        count = self.count(m)
        return k * count + e + self.x * (count - 1 - 2 * e)

    def locals(self, m):
        copies, first = [], 0
        for n, part in enumerate(self.ins[m]):
            height = part.shape[1]
            count = self.count(m)
            here = self.slots[m].at[pl.ds(self.own * count, count), pl.ds(first, height)]
            copies.append(pltpu.make_async_copy(part, here, self.local_sems.at[m, n]))
            first += height
        return copies

    def copy(self, m, c, way):
        piece = self.slots[m].at[c]
        recv_sem = self.side_sems.at[m] if way == OVER_X else self.recv_sems[m].at[c]
        return pltpu.make_async_remote_copy(
            src_ref=piece,
            dst_ref=piece,
            send_sem=self.send_sems.at[m, way],
            recv_sem=recv_sem,
            device_id=self.target(way),
            device_id_type=MESH,
        )

    def spread(self, m, k, e, ways):
        c = self.chunk(m, k, e)
        for way, wanted in ways:
            pl.when(wanted)(lambda way=way: self.copy(m, c, way).start())

    def start_local(self):
        for m in range(len(self.ins)):
            for part in self.locals(m):
                part.start()

    def start_own(self, m):
        for part in self.locals(m):
            part.wait()
        up, down = self.along(m, self.z + 1), self.along(m, self.z - 1)
        across = self.across(m, 0)

        def step(e, carry):
            self.spread(
                m,
                self.own,
                e,
                (
                    (UP, jnp.logical_and(self.has_up, e < up)),
                    (DOWN, jnp.logical_and(self.has_down, e < down)),
                    (OVER_Y, e < across),
                ),
            )
            return carry

        lax.fori_loop(0, self.count(m), step, 0)

    def pieces(self, d):
        below, above = self.z - d, self.z + d
        return (
            (below, below >= 0, self.z + 1, self.has_up, UP),
            (above, jnp.logical_and(d > 0, above < self.depth), self.z - 1, self.has_down, DOWN),
        )

    def arrive_along(self, m, d, e):
        along, across = self.along(m, self.z), self.across(m, d)
        spare = self.count(m) - along
        for at, present, goal, further, way in self.pieces(d):

            @pl.when(jnp.logical_and(present, e < along))
            def _(at=at, goal=goal, further=further, way=way):
                k = at * 2 + self.y
                self.copy(m, self.chunk(m, k, e), UP).wait_recv()
                onward = jnp.logical_and(further, e < self.along(m, goal))
                self.spread(m, k, e, ((way, onward), (OVER_Y, e < across), (OVER_X, e < spare)))

    def arrive_across(self, m, d, e):
        across = self.across(m, d)
        spare = self.count(m) - across
        for at, present, _, _, _ in self.pieces(d):

            @pl.when(jnp.logical_and(present, e < across))
            def _(at=at):
                k = at * 2 + 1 - self.y
                self.copy(m, self.chunk(m, k, e), OVER_Y).wait_recv()
                self.spread(m, k, e, ((OVER_X, e < spare),))

    def slots_of(self, m):
        return self.depth * self.count(m)

    def run(self, m, work=None):
        count = self.count(m)
        ahead = max(self.depth - 1, 0) * count

        def step(t, carry):
            r, e = lax.div(t, count), lax.rem(t, count)
            if m + 1 < len(self.ins):
                pl.when(t == ahead)(lambda: self.start_own(m + 1))
            self.arrive_along(m, r + 1, e)
            self.arrive_across(m, r, e)
            if work is not None:
                work(t)
            return carry

        lax.fori_loop(0, self.slots_of(m), step, 0)

    def totals(self, m, z):
        count, last = self.count(m), self.depth - 1
        least = count - count // 4

        def along(at):
            return least if at in (0, last) else count

        def across(d):
            return min(max(count // 2 + d - 1, count // 2), least) if z in (0, last) else count // 2

        distances = [0, *range(1, z + 1), *range(1, last - z + 1)]
        totals = [0] * 4
        if z < last:
            totals[UP] = along(z + 1) + z * min(along(z), along(z + 1))
        if z > 0:
            totals[DOWN] = along(z - 1) + (last - z) * min(along(z), along(z - 1))
        totals[OVER_Y] = sum(across(d) for d in distances)
        totals[OVER_X] = last * (count - along(z)) + sum(count - across(d) for d in distances)
        return totals

    def all_of(self, m, way, size):
        chunks = self.slots[m].at[pl.ds(0, size)]
        return pltpu.make_async_remote_copy(
            src_ref=chunks,
            dst_ref=chunks,
            send_sem=self.send_sems.at[m, way],
            recv_sem=self.side_sems.at[m],
            device_id=self.target(way),
            device_id_type=MESH,
        )

    def each_place(self, visit):
        for z in range(self.depth):
            pl.when(self.z == z)(lambda z=z: visit(z))

    def settle(self, m):
        self.each_place(lambda z: self.all_of(m, OVER_X, self.totals(m, z)[OVER_X]).wait_recv())

    def drain(self, m):
        def visit(z):
            for way, size in enumerate(self.totals(m, z)):
                if size:
                    self.all_of(m, way, size).wait_send()

        self.each_place(visit)


def gather_sems(total, parts, counts):
    dma = pltpu.SemaphoreType.DMA
    return [dma((len(counts), parts)), dma((len(counts),)), dma((len(counts), 4))] + [
        dma((total * count,)) for count in counts
    ]


def gather_kernel(depth, count, *refs):
    ins, slots = [(ref,) for ref in refs[:count]], refs[count : 2 * count]
    sems = refs[2 * count :]
    gather = Gather(depth, ins, slots, *sems[:3], sems[3:])
    gather.start_local()
    gather.barrier()
    gather.start_own(0)
    for m in range(count):
        gather.run(m)
    for m in range(count):
        gather.settle(m)
        gather.drain(m)


def gather_all(blocks):
    total = lax.axis_size("fs")
    count = len(blocks)
    outs = [jax.ShapeDtypeStruct((total * b.shape[0], *b.shape[1:]), b.dtype) for b in blocks]
    return pl.pallas_call(
        functools.partial(gather_kernel, total // 2, count),
        out_shape=outs,
        in_specs=[pl.BlockSpec(memory_space=pl.ANY)] * count,
        out_specs=[pl.BlockSpec(memory_space=pltpu.VMEM)] * count,
        scratch_shapes=gather_sems(total, 1, [b.shape[0] for b in blocks]),
        compiler_params=pltpu.CompilerParams(
            collective_id=0, has_side_effects=True, vmem_limit_bytes=48 * 2**20
        ),
        name="gather_all",
    )(*blocks)


def hidden_units(gathered, whole_gate, whole_up):
    gate_rows = jnp.dot(gathered, whole_gate, preferred_element_type=jnp.float32)
    up_rows = jnp.dot(gathered, whole_up, preferred_element_type=jnp.float32)
    return (jax.nn.silu(gate_rows) * up_rows).astype(jnp.bfloat16)


def columns_of(blocks):
    return blocks.transpose(1, 0, 2).reshape(blocks.shape[1], -1)


def causal_taps(glu, kernel):
    length = glu.shape[0]
    taps = kernel.shape[0]
    padded = jnp.pad(glu, ((taps - 1, 0), (0, 0)))
    output = jnp.zeros_like(glu)
    for tap_index in range(taps):
        output = output + padded[tap_index : tap_index + length] * kernel[tap_index]
    return output


def chunked(block, pieces):
    return block.reshape(pieces, block.shape[0] // pieces, block.shape[1])


class Layer:
    def __init__(self, gather, tokens, gains, taps, out, scratch):
        self.gather = gather
        self.out = out
        (
            self.own,
            self.stream,
            self.rows,
            self.hidden,
            self.partial,
            self.landed,
            self.padded,
            self.conv,
            self.sums,
            self.act,
            self.mixed,
            *self.packed,
            self.packed_taps,
            self.gains,
            self.gain,
            self.taps,
            self.own_sems,
            self.row_send,
            self.row_recv,
            self.part_send,
            self.part_recv,
            self.sum_send,
            self.sum_recv,
            self.out_sem,
        ) = scratch
        self.half, self.width = self.own.shape
        self.units = self.hidden.shape[1]
        self.total = gather.depth * 2
        self.piece = self.width // self.total
        self.blocks = self.half // ROW_BLOCK
        self.tp = lax.axis_index("tp")
        self.partner = {"tp": 1 - self.tp}
        self.mine = pl.multiple_of(self.tp * self.half, self.half)
        self.theirs = pl.multiple_of((1 - self.tp) * self.half, self.half)
        inputs = (tokens, *gains, taps)
        self.loads = [
            pltpu.make_async_copy(src, dst, self.own_sems.at[n])
            for n, (src, dst) in enumerate(zip(inputs, (self.own, *self.packed, self.packed_taps)))
        ]

    def expand(self):
        for n, packed in enumerate(self.packed):
            target = self.gain if n == 3 else self.gains.at[n]
            for j in range(packed.shape[0]):
                row = packed[j : j + 1, :].astype(jnp.float32)
                target[:, j * LANES : (j + 1) * LANES] = jnp.broadcast_to(row, (SUBLANES, LANES))
        for j in range(self.taps.shape[0]):
            row = self.packed_taps[j : j + 1, :].astype(jnp.float32)
            self.taps[j] = jnp.broadcast_to(row, (SUBLANES, row.shape[1]))

    def remote(self, src, dst, send_sem, recv_sem):
        return pltpu.make_async_remote_copy(
            src_ref=src,
            dst_ref=dst,
            send_sem=send_sem,
            recv_sem=recv_sem,
            device_id=self.partner,
            device_id_type=MESH,
        )

    def row_copy(self, n, first, count):
        here = self.rows.at[n, pl.ds(first, count)]
        return self.remote(here, here, self.row_send.at[n], self.row_recv.at[n])

    def await_rows(self, n):
        self.row_copy(n, self.theirs, self.half).wait_recv()

    def part_copy(self, n, k, width=None):
        cols = pl.ds(pl.multiple_of(k * self.piece, self.piece), self.piece if width is None else width)
        return self.remote(
            self.partial.at[n, pl.ds(self.theirs, self.half), cols],
            self.landed.at[n, :, cols],
            self.part_send.at[n],
            self.part_recv.at[n + (k if n == 2 else 0)],
        )

    def sum_copy(self):
        return self.remote(self.sums.at[0], self.sums.at[1], self.sum_send.at[0], self.sum_recv.at[0])

    def norm(self, n, i, stream):
        square_mean = jnp.mean(stream * stream, axis=-1, keepdims=True)
        scaled = (stream * lax.rsqrt(square_mean + ROW_EPS)).reshape(-1, SUBLANES, self.width) * self.gains[n][None]
        rows = pl.ds(self.mine + self.block(i), ROW_BLOCK)
        self.rows[n, rows, :] = scaled.reshape(stream.shape).astype(jnp.bfloat16)
        self.row_copy(n, self.mine + self.block(i), ROW_BLOCK).start()

    def block(self, i):
        return pl.multiple_of(i * ROW_BLOCK, ROW_BLOCK)

    def start_rows(self):
        def step(i, carry):
            self.norm(0, i, self.own[pl.ds(self.block(i), ROW_BLOCK), :].astype(jnp.float32))
            return carry

        lax.fori_loop(0, self.blocks, step, 0)

    def update(self, n, i, scale):
        first = self.block(i)
        here = pl.ds(first, ROW_BLOCK)
        before = self.own[here, :].astype(jnp.float32) if n == 0 else self.stream[here, :]
        added = self.partial[n, pl.ds(self.mine + first, ROW_BLOCK), :].astype(jnp.float32) + self.landed[
            n, here, :
        ].astype(jnp.float32)
        stream = before + (added if scale is None else scale * added)
        self.stream[here, :] = stream
        self.norm(n + 1, i, stream)

    def await_parts(self, n):
        self.part_copy(n, 0, self.width).wait_recv()

    def matrix(self, m, first, size):
        return self.gather.slots[m][:, :, pl.ds(first, size)].reshape(self.width, size)

    def columns(self, m, k):
        count = self.gather.count(m)
        return self.gather.slots[m][pl.ds(k * count, count)].reshape(-1, self.piece)

    def hidden_tile(self, n, row, height, first, size):
        rows = self.rows[n, pl.ds(row, height), :]
        gate = jnp.dot(rows, self.matrix(0, first, size), preferred_element_type=jnp.float32)
        up = jnp.dot(rows, self.matrix(1, first, size), preferred_element_type=jnp.float32)
        self.hidden[pl.ds(row, height), pl.ds(first, size)] = (jax.nn.silu(gate) * up).astype(jnp.bfloat16)

    def down_piece(self, n, k):
        weights = self.columns(2, k)
        result = jnp.dot(self.hidden[...], weights, preferred_element_type=jnp.float32)
        cols = pl.ds(pl.multiple_of(k * self.piece, self.piece), self.piece)
        self.partial[n, :, cols] = result.astype(jnp.bfloat16)
        self.part_copy(n, k).start()

    def first_work(self, t):
        j = t - FIRST_SLOT

        @pl.when(j == 0)
        def _():
            self.gather.settle(0)
            self.gather.settle(1)
            self.await_rows(0)

        @pl.when(jnp.logical_and(j >= 0, j < self.units // LANES))
        def _():
            self.hidden_tile(0, 0, 2 * self.half, pl.multiple_of(j * LANES, LANES), LANES)

    def second_work(self, t):
        pl.when(t == SECOND_SLOT)(lambda: self.gather.settle(2))

        def step(u, carry):
            j = (t - SECOND_SLOT) * PER_SLOT + u
            i = j - self.total
            pl.when(jnp.logical_and(j >= 0, i < 0))(lambda: self.down_piece(0, j))
            pl.when(i == 0)(lambda: self.await_parts(0))
            pl.when(jnp.logical_and(i >= 0, i < self.blocks))(lambda: self.update(0, i, 0.5))
            return carry

        lax.fori_loop(0, PER_SLOT, step, 0)

    def third_work(self, t):
        blocks = 2 * self.half // CONV_BLOCK

        def step(u, carry):
            j = (t - THIRD_SLOT) * PER_SLOT + u
            i = j - 2

            @pl.when(jnp.logical_or(j == 0, j == 1))
            def _():
                pl.when(j == 0)(lambda: self.gather.settle(3))
                pl.when(j == 1)(lambda: self.await_rows(1))
                self.gated(pl.multiple_of(jnp.where(j == 0, self.mine, self.theirs), self.half))

            pl.when(jnp.logical_and(i >= 0, i < blocks))(lambda: self.convolve(i))
            pl.when(i == blocks)(lambda: self.sum_copy().start())
            return carry

        lax.fori_loop(0, PER_SLOT, step, 0)

    def gated(self, row):
        rows = self.rows[1, pl.ds(row, self.half), :]
        whole = self.gather.slots[3]
        height = whole.shape[1] // 2
        value = whole[:, :height, :].reshape(self.width, -1)
        gate = whole[:, height:, :].reshape(self.width, -1)
        values = jnp.dot(rows, value, preferred_element_type=jnp.float32)
        gates = jnp.dot(rows, gate, preferred_element_type=jnp.float32)
        self.padded[pl.ds(PAD + row, self.half), :] = values * jax.nn.sigmoid(gates)

    def convolve(self, i):
        taps = self.taps.shape[0]
        lanes = self.sums.shape[-1]
        first = pl.multiple_of(i * CONV_BLOCK, CONV_BLOCK)
        window = self.padded[pl.ds(first, CONV_BLOCK + PAD), :]
        channels = window.shape[1]
        total = jnp.zeros((CONV_BLOCK // SUBLANES, SUBLANES, channels), jnp.float32)
        offsets = [PAD - (taps - 1) + j for j in range(taps)]
        for shift in range(SUBLANES):
            mine = [(j, at) for j, at in enumerate(offsets) if at % SUBLANES == shift]
            reach = max(at for _, at in mine) - shift + CONV_BLOCK
            shifted = window[shift : shift + reach]
            for j, at in mine:
                block = shifted[at - shift : at - shift + CONV_BLOCK].reshape(total.shape)
                total = total + block * self.taps[j][None]
        total = total.reshape(CONV_BLOCK, channels)
        here = pl.ds(first, CONV_BLOCK)
        self.conv[here, :] = total
        plain = jnp.sum(total, axis=-1, keepdims=True)
        squared = jnp.sum(total * total, axis=-1, keepdims=True)
        lane = lax.broadcasted_iota(jnp.int32, (CONV_BLOCK, lanes), 1)
        self.sums[0, here, :] = jnp.where(lane < lanes // 2, plain, squared)

    def activate(self):
        lanes = self.sums.shape[-1]
        channels = 2 * self.conv.shape[1]

        def step(i, carry):
            here = pl.ds(pl.multiple_of(i * CONV_BLOCK, CONV_BLOCK), CONV_BLOCK)
            sums = (self.sums[0, here, :] + self.sums[1, here, :]) / channels
            average, square = sums[:, :1], sums[:, lanes // 2 : lanes // 2 + 1]
            spread = jnp.maximum(square - average * average, 0.0)
            scaled = (self.conv[here, :] - average) * lax.rsqrt(spread + CHAN_EPS)
            scaled = scaled.reshape(-1, SUBLANES, scaled.shape[1]) * self.gain[...][None]
            self.act[here, :] = jax.nn.silu(scaled.reshape(CONV_BLOCK, -1)).astype(jnp.bfloat16)
            return carry

        lax.fori_loop(0, 2 * self.half // CONV_BLOCK, step, 0)

    def mix(self):
        def step(k, carry):
            weights = self.columns(4, k)
            result = jnp.dot(self.act[...], weights, preferred_element_type=jnp.float32)
            cols = pl.ds(pl.multiple_of(k * self.piece, self.piece), self.piece)
            self.partial[1, :, cols] = result.astype(jnp.bfloat16)
            self.part_copy(1, k).start()
            return carry

        lax.fori_loop(0, self.total, step, 0)

    def finish_conv(self):
        self.sum_copy().wait_recv()
        self.activate()
        self.gather.settle(4)
        self.mix()
        self.await_parts(1)

        def step(i, carry):
            self.update(1, i, None)
            return carry

        lax.fori_loop(0, self.blocks, step, 0)

    def second_half_step(self):
        tile = 2 * LANES
        whole = self.units // tile
        early = min(2, whole)

        def split(i, carry):
            pl.when(i == early)(lambda: self.await_rows(2))
            row = jnp.where(i < early, self.mine, self.theirs)
            first = pl.multiple_of(lax.rem(i, early) * tile, tile)
            self.hidden_tile(2, pl.multiple_of(row, self.half), self.half, first, tile)
            return carry

        lax.fori_loop(0, 2 * early, split, 0)

        def step(j, carry):
            self.hidden_tile(2, 0, 2 * self.half, pl.multiple_of(j * tile, tile), tile)
            return carry

        lax.fori_loop(early, whole, step, 0)
        if self.units % tile:
            self.hidden_tile(2, 0, 2 * self.half, whole * tile, self.units % tile)

        def piece(k, carry):
            self.down_piece(2, k)
            return carry

        lax.fori_loop(0, self.total, piece, 0)

        def finish(k, carry):
            self.part_copy(2, k).wait_recv()
            cols = pl.ds(pl.multiple_of(k * self.piece, self.piece), self.piece)
            added = self.partial[2, pl.ds(self.mine, self.half), cols].astype(jnp.float32) + self.landed[
                2, :, cols
            ].astype(jnp.float32)
            self.mixed[:, cols] = (self.stream[:, cols] + 0.5 * added).astype(self.mixed.dtype)
            pltpu.make_async_copy(self.mixed.at[:, cols], self.out.at[:, cols], self.out_sem.at[0]).start()
            return carry

        lax.fori_loop(0, self.total, finish, 0)

    def drain(self):
        self.sum_copy().wait_send()
        for n in range(3):
            self.row_copy(n, self.mine, self.half).wait_send()
            self.part_copy(n, 0, self.width).wait_send()

    def run(self):
        gather = self.gather
        gather.start_local()
        for load in self.loads:
            load.start()
        gather.barrier(self.partner)
        gather.start_own(0)
        for load in self.loads:
            load.wait()
        self.expand()
        self.start_rows()
        self.padded[:PAD, :] = jnp.zeros((PAD, self.padded.shape[1]), jnp.float32)
        gather.run(0)
        gather.run(1)
        gather.run(2, self.first_work)
        gather.run(3, self.second_work)
        gather.run(4, self.third_work)
        self.finish_conv()
        self.second_half_step()
        for m in range(len(gather.ins)):
            gather.drain(m)
        self.drain()
        pltpu.make_async_copy(self.mixed, self.out, self.out_sem.at[0]).wait()


def layer_kernel(depth, *refs):
    tokens, gains, taps, refs = refs[0], refs[1:5], refs[5], refs[6:]
    ins, refs = ((refs[0],), (refs[1],), (refs[2],), refs[3:5], (refs[5],)), refs[6:]
    out, refs = refs[0], refs[1:]
    slots, sems, scratch = refs[:5], refs[5:13], refs[13:]
    gather = Gather(depth, ins, slots, *sems[:3], sems[3:])
    Layer(gather, tokens, gains, taps, out, scratch).run()


def fused_layer(tokens, gains, depthwise, blocks, smalls):
    total = lax.axis_size("fs")
    half, width = tokens.shape
    units, (taps, channels) = blocks[0].shape[2], depthwise.shape
    vmem, dma = pltpu.VMEM, pltpu.SemaphoreType.DMA
    count, height, piece = smalls[0].shape
    shapes = [b.shape for b in blocks] + [(count, 2 * height, piece), (count, height, piece)]
    f32, bf16 = jnp.float32, jnp.bfloat16
    return pl.pallas_call(
        functools.partial(layer_kernel, total // 2),
        out_shape=jax.ShapeDtypeStruct((half, width), bf16),
        in_specs=[pl.BlockSpec(memory_space=pltpu.HBM)] * 12,
        out_specs=pl.BlockSpec(memory_space=pltpu.HBM),
        scratch_shapes=[vmem((total * shape[0], *shape[1:]), bf16) for shape in shapes]
        + gather_sems(total, 2, [shape[0] for shape in shapes])
        + [
            vmem((half, width), bf16),
            vmem((half, width), f32),
            vmem((3, 2 * half, width), bf16),
            vmem((2 * half, units), bf16),
            vmem((3, 2 * half, width), bf16),
            vmem((3, half, width), bf16),
            vmem((PAD + 2 * half, channels), f32),
            vmem((2 * half, channels), f32),
            vmem((2, 2 * half, LANES), f32),
            vmem((2 * half, channels), bf16),
            vmem((half, width), bf16),
        ]
        + [vmem(gain.shape, bf16) for gain in gains]
        + [
            vmem(depthwise.shape, bf16),
            vmem((3, SUBLANES, width), f32),
            vmem((SUBLANES, channels), f32),
            vmem((taps, SUBLANES, channels), f32),
            dma((6,)),
            dma((3,)),
            dma((3,)),
            dma((3,)),
            dma((2 + total,)),
            dma((1,)),
            dma((1,)),
            dma((1,)),
        ],
        compiler_params=pltpu.CompilerParams(
            collective_id=0, has_side_effects=True, vmem_limit_bytes=58 * 2**20
        ),
        name="fused_layer",
    )(tokens, *gains, depthwise, *blocks, *smalls)


def fits(half, ffn_gate, ffn_down, conv_value, conv_out, depthwise):
    piece, total = ffn_gate.shape[0], lax.axis_size("fs")
    slots, conv_slots = total // 2 * CHUNKS, total // 2 * CONV_CHUNKS
    return (
        piece % (16 * CHUNKS) == 0
        and ffn_down.shape[0] % (16 * CHUNKS) == 0
        and conv_out.shape[0] == piece
        and conv_value.shape[1] == piece
        and piece % LANES == 0
        and ffn_gate.shape[1] % LANES == 0
        and half % ROW_BLOCK == 0
        and half % CONV_BLOCK == 0
        and depthwise.shape[0] <= PAD
        and slots >= FIRST_SLOT + ffn_gate.shape[1] // LANES
        and (conv_slots - SECOND_SLOT) * PER_SLOT >= total + half // ROW_BLOCK
        and (conv_slots - THIRD_SLOT) * PER_SLOT > 2 + 2 * half // CONV_BLOCK
        and lax.axis_size("tp") == 2
        and lax.axis_size("rep") == 2
    )


def shards(
    tokens,
    norm_first,
    norm_mixer,
    norm_second,
    ffn_gate,
    ffn_up,
    ffn_down,
    conv_value,
    conv_gate,
    depthwise,
    conv_gain,
    conv_out,
):
    width = tokens.shape[-1]
    if fits(tokens.size // width, ffn_gate, ffn_down, conv_value, conv_out, depthwise):
        mixed = fused_layer(
            tokens.reshape(-1, width),
            [gain.reshape(-1, LANES) for gain in (norm_first, norm_mixer, norm_second, conv_gain)],
            depthwise,
            [chunked(block, CHUNKS) for block in (ffn_gate, ffn_up, ffn_down)],
            [chunked(block, CONV_CHUNKS) for block in (conv_value, conv_gate, conv_out)],
        )
        return mixed.reshape(tokens.shape)
    stream = tokens.reshape(-1, width).astype(jnp.float32)
    first_rows = widen(rms_rows(stream, norm_first))
    small = jnp.concatenate([conv_value, conv_gate, conv_out.reshape(-1, conv_value.shape[1])])
    gate, up, down, small_all = gather_all(
        [chunked(block, CHUNKS) for block in (ffn_gate, ffn_up, ffn_down, small)]
    )
    whole_gate = gate.reshape(-1, gate.shape[-1])
    whole_up = up.reshape(-1, up.shape[-1])
    total = lax.axis_size("fs")
    whole_down = columns_of(down.reshape(total, -1, down.shape[-1]))
    small_all = small_all.reshape(total, -1, small_all.shape[-1])
    rows = conv_value.shape[0]
    channels_here = conv_value.shape[1]
    whole_value = small_all[:, :rows].reshape(-1, channels_here)
    whole_conv_gate = small_all[:, rows : 2 * rows].reshape(-1, channels_here)
    whole_out = columns_of(small_all[:, 2 * rows :].reshape(total, *conv_out.shape))

    hidden = hidden_units(first_rows, whole_gate, whole_up)
    stream = stream + 0.5 * narrow(jnp.dot(hidden, whole_down, preferred_element_type=jnp.float32))
    gathered = widen(rms_rows(stream, norm_mixer))
    values = jnp.dot(gathered, whole_value, preferred_element_type=jnp.float32)
    gates = jnp.dot(gathered, whole_conv_gate, preferred_element_type=jnp.float32)
    glu = reorder(values * jax.nn.sigmoid(gates))
    conv = causal_taps(glu, depthwise.astype(jnp.float32))
    channels = conv.shape[1] * lax.axis_size("tp")
    sums, squares = lax.psum((jnp.sum(conv, axis=1), jnp.sum(conv * conv, axis=1)), "tp")
    average = sums / channels
    spread = jnp.maximum(squares / channels - average * average, 0.0)
    centred = conv - average[:, None]
    activated = jax.nn.silu(
        centred * lax.rsqrt(spread[:, None] + CHAN_EPS) * conv_gain.astype(jnp.float32)
    ).astype(jnp.bfloat16)
    stream = stream + narrow(jnp.dot(reorder(activated), whole_out, preferred_element_type=jnp.float32))
    second_rows = widen(rms_rows(stream, norm_second))
    second_hidden = hidden_units(second_rows, whole_gate, whole_up)
    stream = stream + 0.5 * narrow(jnp.dot(second_hidden, whole_down, preferred_element_type=jnp.float32))
    return stream.astype(jnp.bfloat16).reshape(tokens.shape)


def solution(mesh):
    in_specs = (
        P(("rep", "fs"), "tp", None),
        P(),
        P(),
        P(),
        P("fs", "tp"),
        P("fs", "tp"),
        P("tp", "fs"),
        P("fs", "tp"),
        P("fs", "tp"),
        P(None, "tp"),
        P("tp"),
        P("tp", "fs"),
    )
    out_specs = P(("rep", "fs"), "tp", None)
    return jax.shard_map(shards, mesh=mesh, in_specs=in_specs, out_specs=out_specs, check_vma=False)
```

time: 188 us -> 171 us (0.910)
  Pallas kernels: 182 us -> 168 us
  local copies, waits for them, and re-layouts: 5.53 us -> 2.3 us
    pallas_call x1, Pallas kernels: 182 us -> 168 us  [fused_layer(): pl.pallas_call(functools.partial(layer_kernel, total // 2), out_shape=jax...]
    reshape x4 -> x0, local copies, waits for them, and re-layouts: 2.39 us -> none  [the longest x3 1.82 us: shards(): gain.reshape(1, -1)]
where the time goes in v3:
time: 171 us
  Pallas kernels  168 us (98%)
  local copies, waits for them, and re-layouts  2.3 us (1%)
    pallas_call x1, Pallas kernels, fused_layer(): pl.pallas_call(functools.partial(layer_kernel, total // 2), out_shape=jax...  168 us

profile of v3, /device:TPU:0, one launch (start us, length us, event | category | flops | bytes accessed | tf_op | source)
XLA Modules:
  0.0 170.5 jit_solution(16334024039628015242)
XLA Ops:
  0.0 168.2 %fused_layer.1 = bf16[256,2048]{1,0:T(8,128)(2,1)} custom-call(bf16[256,2048]{1,0:T(8,128)(2,1)} %bitcast.13, bf16[16,128]{1,0:T(8,128)(2,1)} %bitcast.20, bf16[16,128]{1,0:T(8,128)(2,1)} %bitcast.21, bf16[16,128]{1,0:T(8,128)(2,1)} %bitcast.22, bf16[2,128]{1,0:T(2,128)(2,1)} %bitcast.23, bf16[31,256]{1,0:T(8,128)(2,1)} %refs_5_.1, ...), custom_call_target="tpu_custom_call" | custom-call | tf_op jit(solution)/shard_map/fused_layer/pallas_call | solution.py:663
  168.2 2.3 %copy.14 = bf16[1,256,2048]{2,1,0:T(8,128)(2,1)} copy(bf16[1,256,2048]{2,1,0:T(8,128)(2,1)} %bitcast.12) | data formatting | bytes 2097152

commit v4 on v3

--- a/solution.py
+++ b/solution.py
@@ -21,6 +21,9 @@
 SECOND_SLOT = 2
 THIRD_SLOT = 2
 PER_SLOT = 2
+SUM_WAIT = 4
+MIX_GROUP = 4
+DOWN_GROUP = 2
 UP, DOWN, OVER_X, OVER_Y = range(4)
 
 
@@ -495,6 +498,9 @@
 
             pl.when(jnp.logical_and(i >= 0, i < blocks))(lambda: self.convolve(i))
             pl.when(i == blocks)(lambda: self.sum_copy().start())
+            i = i - blocks - SUM_WAIT
+            pl.when(i == 0)(lambda: self.sum_copy().wait_recv())
+            pl.when(jnp.logical_and(i >= 0, i < blocks))(lambda: self.activate(i))
             return carry
 
         lax.fori_loop(0, PER_SLOT, step, 0)
@@ -532,38 +538,40 @@
         lane = lax.broadcasted_iota(jnp.int32, (CONV_BLOCK, lanes), 1)
         self.sums[0, here, :] = jnp.where(lane < lanes // 2, plain, squared)
 
-    def activate(self):
+    def activate(self, i):
         lanes = self.sums.shape[-1]
         channels = 2 * self.conv.shape[1]
-
-        def step(i, carry):
-            here = pl.ds(pl.multiple_of(i * CONV_BLOCK, CONV_BLOCK), CONV_BLOCK)
-            sums = (self.sums[0, here, :] + self.sums[1, here, :]) / channels
-            average, square = sums[:, :1], sums[:, lanes // 2 : lanes // 2 + 1]
-            spread = jnp.maximum(square - average * average, 0.0)
-            scaled = (self.conv[here, :] - average) * lax.rsqrt(spread + CHAN_EPS)
-            scaled = scaled.reshape(-1, SUBLANES, scaled.shape[1]) * self.gain[...][None]
-            self.act[here, :] = jax.nn.silu(scaled.reshape(CONV_BLOCK, -1)).astype(jnp.bfloat16)
-            return carry
-
-        lax.fori_loop(0, 2 * self.half // CONV_BLOCK, step, 0)
-
-    def mix(self):
-        def step(k, carry):
-            weights = self.columns(4, k)
-            result = jnp.dot(self.act[...], weights, preferred_element_type=jnp.float32)
-            cols = pl.ds(pl.multiple_of(k * self.piece, self.piece), self.piece)
-            self.partial[1, :, cols] = result.astype(jnp.bfloat16)
-            self.part_copy(1, k).start()
-            return carry
-
-        lax.fori_loop(0, self.total, step, 0)
+        here = pl.ds(pl.multiple_of(i * CONV_BLOCK, CONV_BLOCK), CONV_BLOCK)
+        sums = (self.sums[0, here, :] + self.sums[1, here, :]) / channels
+        average, square = sums[:, :1], sums[:, lanes // 2 : lanes // 2 + 1]
+        spread = jnp.maximum(square - average * average, 0.0)
+        scaled = (self.conv[here, :] - average) * lax.rsqrt(spread + CHAN_EPS)
+        scaled = scaled.reshape(-1, SUBLANES, scaled.shape[1]) * self.gain[...][None]
+        self.act[here, :] = jax.nn.silu(scaled.reshape(CONV_BLOCK, -1)).astype(jnp.bfloat16)
+
+    def mix(self, row, k):
+        rows, cols = pl.ds(row, self.half), pl.ds(pl.multiple_of(k * self.piece, self.piece), self.piece)
+        result = jnp.dot(self.act[rows, :], self.columns(4, k), preferred_element_type=jnp.float32)
+        self.partial[1, rows, cols] = result.astype(jnp.bfloat16)
 
     def finish_conv(self):
-        self.sum_copy().wait_recv()
-        self.activate()
         self.gather.settle(4)
-        self.mix()
+
+        def theirs(g, carry):
+            group = [g * MIX_GROUP + u for u in range(MIX_GROUP)]
+            for k in group:
+                self.mix(self.theirs, k)
+            for k in group:
+                self.part_copy(1, k).start()
+            return carry
+
+        def mine(g, carry):
+            for u in range(MIX_GROUP):
+                self.mix(self.mine, g * MIX_GROUP + u)
+            return carry
+
+        lax.fori_loop(0, self.total // MIX_GROUP, theirs, 0)
+        lax.fori_loop(0, self.total // MIX_GROUP, mine, 0)
         self.await_parts(1)
 
         def step(i, carry):
@@ -594,23 +602,36 @@
         if self.units % tile:
             self.hidden_tile(2, 0, 2 * self.half, whole * tile, self.units % tile)
 
-        def piece(k, carry):
-            self.down_piece(2, k)
-            return carry
-
-        lax.fori_loop(0, self.total, piece, 0)
-
-        def finish(k, carry):
-            self.part_copy(2, k).wait_recv()
-            cols = pl.ds(pl.multiple_of(k * self.piece, self.piece), self.piece)
-            added = self.partial[2, pl.ds(self.mine, self.half), cols].astype(jnp.float32) + self.landed[
-                2, :, cols
-            ].astype(jnp.float32)
-            self.mixed[:, cols] = (self.stream[:, cols] + 0.5 * added).astype(self.mixed.dtype)
-            pltpu.make_async_copy(self.mixed.at[:, cols], self.out.at[:, cols], self.out_sem.at[0]).start()
-            return carry
-
-        lax.fori_loop(0, self.total, finish, 0)
+        def down(row, k):
+            return jnp.dot(self.hidden[pl.ds(row, self.half), :], self.columns(2, k), preferred_element_type=jnp.float32)
+
+        def columns(k):
+            return pl.ds(pl.multiple_of(k * self.piece, self.piece), self.piece)
+
+        def theirs(g, carry):
+            group = [g * DOWN_GROUP + u for u in range(DOWN_GROUP)]
+            for k in group:
+                self.partial[2, pl.ds(self.theirs, self.half), columns(k)] = down(self.theirs, k).astype(jnp.bfloat16)
+            for k in group:
+                self.part_copy(2, k).start()
+            return carry
+
+        def mine(g, carry):
+            group = [g * DOWN_GROUP + u for u in range(DOWN_GROUP)]
+            for k in group:
+                self.part_copy(2, k).wait_recv()
+            for k in group:
+                cols = columns(k)
+                own = down(self.mine, k).astype(jnp.bfloat16).astype(jnp.float32)
+                added = own + self.landed[2, :, cols].astype(jnp.float32)
+                self.mixed[:, cols] = (self.stream[:, cols] + 0.5 * added).astype(self.mixed.dtype)
+            for k in group:
+                cols = columns(k)
+                pltpu.make_async_copy(self.mixed.at[:, cols], self.out.at[:, cols], self.out_sem.at[0]).start()
+            return carry
+
+        lax.fori_loop(0, self.total // DOWN_GROUP, theirs, 0)
+        lax.fori_loop(0, self.total // DOWN_GROUP, mine, 0)
 
     def drain(self):
         self.sum_copy().wait_send()
@@ -715,9 +736,11 @@
         and half % ROW_BLOCK == 0
         and half % CONV_BLOCK == 0
         and depthwise.shape[0] <= PAD
+        and total % MIX_GROUP == 0
+        and total % DOWN_GROUP == 0
         and slots >= FIRST_SLOT + ffn_gate.shape[1] // LANES
         and (conv_slots - SECOND_SLOT) * PER_SLOT >= total + half // ROW_BLOCK
-        and (conv_slots - THIRD_SLOT) * PER_SLOT > 2 + 2 * half // CONV_BLOCK
+        and (conv_slots - THIRD_SLOT) * PER_SLOT >= 2 + SUM_WAIT + 4 * half // CONV_BLOCK
         and lax.axis_size("tp") == 2
         and lax.axis_size("rep") == 2
     )

time: 171 us -> 169 us (0.988)
  no operation moved by 1% of the time
where the time goes in v4:
time: 169 us
  Pallas kernels  167 us (99%)
  local copies, waits for them, and re-layouts  2.3 us (1%)
    pallas_call x1, Pallas kernels, fused_layer(): pl.pallas_call(functools.partial(layer_kernel, total // 2), out_shape=jax...  167 us

profile of v4, /device:TPU:0, one launch (start us, length us, event | category | flops | bytes accessed | tf_op | source)
XLA Modules:
  0.0 169.3 jit_solution(13453344244716284802)
XLA Ops:
  0.0 167.0 %fused_layer.1 = bf16[256,2048]{1,0:T(8,128)(2,1)} custom-call(bf16[256,2048]{1,0:T(8,128)(2,1)} %bitcast.13, bf16[16,128]{1,0:T(8,128)(2,1)} %bitcast.20, bf16[16,128]{1,0:T(8,128)(2,1)} %bitcast.21, bf16[16,128]{1,0:T(8,128)(2,1)} %bitcast.22, bf16[2,128]{1,0:T(2,128)(2,1)} %bitcast.23, bf16[31,256]{1,0:T(8,128)(2,1)} %refs_5_.1, ...), custom_call_target="tpu_custom_call" | custom-call | tf_op jit(solution)/shard_map/fused_layer/pallas_call | solution.py:684
  167.0 2.3 %copy.14 = bf16[1,256,2048]{2,1,0:T(8,128)(2,1)} copy(bf16[1,256,2048]{2,1,0:T(8,128)(2,1)} %bitcast.12) | data formatting | bytes 2097152

commit v5 on v4

--- a/solution.py
+++ b/solution.py
@@ -21,6 +21,7 @@
 SECOND_SLOT = 2
 THIRD_SLOT = 2
 PER_SLOT = 2
+LARGE = 3
 SUM_WAIT = 4
 MIX_GROUP = 4
 DOWN_GROUP = 2
@@ -98,13 +99,19 @@
     def at_end(self, at):
         return jnp.logical_or(at == 0, at == self.depth - 1)
 
+    def least(self, m):
+        count = self.count(m)
+        return count - count // 4 if m < LARGE else count
+
+    def near(self, m):
+        return 1 if m < LARGE else 2
+
     def along(self, m, at):
-        count = self.count(m)
-        return jnp.where(self.at_end(at), count - count // 4, count)
+        return jnp.where(self.at_end(at), self.least(m), self.count(m))
 
     def across(self, m, d):
         count = self.count(m)
-        far = jnp.clip(count // 2 + d - 1, count // 2, count - count // 4)
+        far = jnp.clip(count // 2 + d - self.near(m), count // 2, count - count // 4)
         return jnp.where(self.at_end(self.z), far, count // 2)
 
     def chunk(self, m, k, e):
@@ -199,7 +206,7 @@
 
     def run(self, m, work=None):
         count = self.count(m)
-        ahead = max(self.depth - 1, 0) * count
+        ahead = min(self.depth - 1, 1 if m >= LARGE else self.depth) * count
 
         def step(t, carry):
             r, e = lax.div(t, count), lax.rem(t, count)
@@ -215,13 +222,14 @@
 
     def totals(self, m, z):
         count, last = self.count(m), self.depth - 1
-        least = count - count // 4
+        least = self.least(m)
 
         def along(at):
             return least if at in (0, last) else count
 
         def across(d):
-            return min(max(count // 2 + d - 1, count // 2), least) if z in (0, last) else count // 2
+            far = min(max(count // 2 + d - self.near(m), count // 2), count - count // 4)
+            return far if z in (0, last) else count // 2
 
         distances = [0, *range(1, z + 1), *range(1, last - z + 1)]
         totals = [0] * 4

time: 169 us -> 168 us (level)
  no operation moved by 1% of the time
where the time goes in v5:
time: 168 us
  Pallas kernels  166 us (99%)
  local copies, waits for them, and re-layouts  2.3 us (1%)
    pallas_call x1, Pallas kernels, fused_layer(): pl.pallas_call(functools.partial(layer_kernel, total // 2), out_shape=jax...  166 us

profile of v5, /device:TPU:0, one launch (start us, length us, event | category | flops | bytes accessed | tf_op | source)
XLA Modules:
  0.0 168.3 jit_solution(16180938351143824699)
XLA Ops:
  0.0 166.0 %fused_layer.1 = bf16[256,2048]{1,0:T(8,128)(2,1)} custom-call(bf16[256,2048]{1,0:T(8,128)(2,1)} %bitcast.13, bf16[16,128]{1,0:T(8,128)(2,1)} %bitcast.20, bf16[16,128]{1,0:T(8,128)(2,1)} %bitcast.21, bf16[16,128]{1,0:T(8,128)(2,1)} %bitcast.22, bf16[2,128]{1,0:T(2,128)(2,1)} %bitcast.23, bf16[31,256]{1,0:T(8,128)(2,1)} %refs_5_.1, ...), custom_call_target="tpu_custom_call" | custom-call | tf_op jit(solution)/shard_map/fused_layer/pallas_call | solution.py:692
  166.0 2.3 %copy.14 = bf16[1,256,2048]{2,1,0:T(8,128)(2,1)} copy(bf16[1,256,2048]{2,1,0:T(8,128)(2,1)} %bitcast.12) | data formatting | bytes 2097152

commit v6 on v5

--- a/solution.py
+++ b/solution.py
@@ -268,10 +268,10 @@
         self.each_place(visit)
 
 
-def gather_sems(total, parts, counts):
+def gather_sems(total, parts, counts, large=None):
     dma = pltpu.SemaphoreType.DMA
     return [dma((len(counts), parts)), dma((len(counts),)), dma((len(counts), 4))] + [
-        dma((total * count,)) for count in counts
+        dma((total * count,)) for count in counts[:large]
     ]
 
 
@@ -676,8 +676,8 @@
     tokens, gains, taps, refs = refs[0], refs[1:5], refs[5], refs[6:]
     ins, refs = ((refs[0],), (refs[1],), (refs[2],), refs[3:5], (refs[5],)), refs[6:]
     out, refs = refs[0], refs[1:]
-    slots, sems, scratch = refs[:5], refs[5:13], refs[13:]
-    gather = Gather(depth, ins, slots, *sems[:3], sems[3:])
+    slots, sems, scratch = refs[:5], refs[5:11], refs[11:]
+    gather = Gather(depth, ins, slots, *sems[:3], (*sems[3:], *sems[3:5]))
     Layer(gather, tokens, gains, taps, out, scratch).run()
 
 
@@ -695,7 +695,7 @@
         in_specs=[pl.BlockSpec(memory_space=pltpu.HBM)] * 12,
         out_specs=pl.BlockSpec(memory_space=pltpu.HBM),
         scratch_shapes=[vmem((total * shape[0], *shape[1:]), bf16) for shape in shapes]
-        + gather_sems(total, 2, [shape[0] for shape in shapes])
+        + gather_sems(total, 2, [shape[0] for shape in shapes], LARGE)
         + [
             vmem((half, width), bf16),
             vmem((half, width), f32),

time: 168 us -> 168 us (level)
  no operation moved by 1% of the time
where the time goes in v6:
time: 168 us
  Pallas kernels  165 us (98%)
  local copies, waits for them, and re-layouts  2.3 us (1%)
    pallas_call x1, Pallas kernels, fused_layer(): pl.pallas_call(functools.partial(layer_kernel, total // 2), out_shape=jax...  165 us

profile of v6, /device:TPU:0, one launch (start us, length us, event | category | flops | bytes accessed | tf_op | source)
XLA Modules:
  0.0 167.7 jit_solution(16329105706893710284)
XLA Ops:
  0.0 165.4 %fused_layer.1 = bf16[256,2048]{1,0:T(8,128)(2,1)} custom-call(bf16[256,2048]{1,0:T(8,128)(2,1)} %bitcast.13, bf16[16,128]{1,0:T(8,128)(2,1)} %bitcast.20, bf16[16,128]{1,0:T(8,128)(2,1)} %bitcast.21, bf16[16,128]{1,0:T(8,128)(2,1)} %bitcast.22, bf16[2,128]{1,0:T(2,128)(2,1)} %bitcast.23, bf16[31,256]{1,0:T(8,128)(2,1)} %refs_5_.1, ...), custom_call_target="tpu_custom_call" | custom-call | tf_op jit(solution)/shard_map/fused_layer/pallas_call | solution.py:692
  165.4 2.3 %copy.14 = bf16[1,256,2048]{2,1,0:T(8,128)(2,1)} copy(bf16[1,256,2048]{2,1,0:T(8,128)(2,1)} %bitcast.12) | data formatting | bytes 2097152
